TPU v7x, 32 devices: a whole 2x2x4 slice. The times are simulated.
32 devices in a mesh: sp: 8 (over z, y), tp: 4 (over x, core).
Axes of the slice: x: 2, y: 2, z: 4, core: 2. Of those that a mesh axis runs over, the one named last changes fastest.
Arguments:
- tokens: bfloat16 [3072, 2048], P('sp', 'tp'), may hold values from -6 to 6
- norm_gain: float32 [3, 2048], replicated, may hold values from 0.1 to 1.9
- w_value: bfloat16 [3, 2048, 1024], P(None, 'sp', 'tp'), may hold values from -0.125 to 0.125
- w_gate: bfloat16 [3, 2048, 1024], P(None, 'sp', 'tp'), may hold values from -0.125 to 0.125
- conv_taps: float32 [3, 31, 1024], P(None, None, 'tp'), may hold values from -2.4 to 2.4
- conv_bias: float32 [3, 1024], P(None, 'tp'), may hold values from -3 to 3
- ln_gain: float32 [3, 1024], P(None, 'tp'), may hold values from 0.1 to 1.9
- ln_shift: float32 [3, 1024], P(None, 'tp'), may hold values from -3 to 3
- w_out: bfloat16 [3, 1024, 2048], P(None, 'tp', 'sp'), may hold values from -0.1875 to 0.1875
Outputs:
- stream: bfloat16 [3072, 2048], P('sp', 'tp')
All inputs are finite; a program needn't handle non-finite values.
Results may differ from a plain program's by a relative error of at most 0.015.
Values may be sent and summed in bfloat16 or wider, within the bound.
A program may use at most 64 MiB of HBM per device.

v0:
```python
import functools

import jax
import jax.numpy as jnp
from jax import lax
from jax.experimental import pallas as pl
from jax.experimental.pallas import tpu as pltpu
from jax.sharding import PartitionSpec as P

MESH = pl.DeviceIdType.MESH

norm_floor = 0.01


def with_halo(array, sides, width):
    for axis, dim in sides:
        size, length = (lax.axis_size(axis), array.shape[dim])
        up = [(i, (i + 1) % size) for i in range(size - 1)]
        down = [(j, i) for i, j in up]
        last = lax.slice_in_dim(array, length - width, length, axis=dim)
        first = lax.slice_in_dim(array, 0, width, axis=dim)
        before = lax.ppermute(last, axis, up)
        after = lax.ppermute(first, axis, down)
        array = jnp.concatenate([before, array, after], axis=dim)
    return array


def body(tokens, norm_gain, w_value, w_gate, conv_taps, conv_bias, ln_gain, ln_shift, w_out):
    stream = tokens
    layer_count = w_value.shape[0]
    reach = conv_taps.shape[1] // 2
    local_channels = w_value.shape[2]
    channels = local_channels * lax.axis_size("tp")
    tok_rows = tokens.shape[0]
    whole_value, whole_gate = (
        lax.all_gather(w_value, "sp", axis=1, tiled=True),
        lax.all_gather(w_gate, "sp", axis=1, tiled=True),
    )
    whole_out = lax.all_gather(w_out, "sp", axis=2, tiled=True)
    for layer_index in range(layer_count):
        whole_rows = lax.all_gather(stream, "tp", axis=1, tiled=True)
        rows_f32 = whole_rows.astype(jnp.float32)
        scale_rows = lax.rsqrt(jnp.mean(rows_f32 * rows_f32, axis=-1, keepdims=True) + norm_floor)
        normed = (rows_f32 * scale_rows * norm_gain[layer_index]).astype(jnp.bfloat16)
        value_rows = jnp.dot(normed, whole_value[layer_index], preferred_element_type=jnp.float32)
        gate_rows = jnp.dot(normed, whole_gate[layer_index], preferred_element_type=jnp.float32)
        gated_input = (value_rows * jax.nn.sigmoid(gate_rows)).astype(jnp.bfloat16)
        padded = with_halo(gated_input, (("sp", 0),), reach)
        padded = padded.astype(jnp.float32)
        convolved = jnp.zeros((tok_rows, local_channels), jnp.float32) + conv_bias[layer_index]
        for offset in range(2 * reach + 1):
            convolved = (
                convolved + conv_taps[layer_index, offset] * padded[offset : offset + tok_rows]
            )
        moments = lax.psum(
            (
                jnp.sum(convolved, axis=-1, keepdims=True),
                jnp.sum(convolved * convolved, axis=-1, keepdims=True),
            ),
            "tp",
        )
        average = moments[0] / channels
        spread = moments[1] / channels - average * average
        activated = jax.nn.silu(
            (convolved - average) * lax.rsqrt(spread + norm_floor) * ln_gain[layer_index]
            + ln_shift[layer_index]
        ).astype(jnp.bfloat16)
        partial_rows = jnp.dot(
            activated, whole_out[layer_index], preferred_element_type=jnp.float32
        )
        summed = lax.psum_scatter(
            partial_rows.astype(jnp.bfloat16), "tp", scatter_dimension=1, tiled=True
        ).astype(jnp.float32)
        stream = (stream.astype(jnp.float32) + summed).astype(jnp.bfloat16)
    return stream


def ring_order(layers, m):
    order = [(0, 0, 1), (0, 1, 1)]
    for layer in range(layers):
        order.append((layer, 2, 1))
        for step in range(2, m + 1):
            order += [(layer, 0, step), (layer, 1, step)]
        ahead = [(layer + 1, 0, 1), (layer + 1, 1, 1)] if layer + 1 < layers else []
        for step in range(2, m + 1):
            order.append((layer, 2, step))
            order += ahead[:1]
            ahead = ahead[1:]
        order += ahead
    if m > 2:
        last = layers - 1
        early = [(last, 2, step) for step in range(2, m - 1)]
        order = [e for e in order if e not in early]
        for e in early:
            order.insert(order.index((last, 1, e[2] + 1)), e)
    return order


def fused(
    dims,
    tok, gain_in, wv_in, wg_in, wo_in, taps_in, bias_in, lng_in, lns_in,
    out,
    wvg, wo, taps, bias, lng, lns, stream, gated, conv, acc1, acc2, act,
    part_out, part_in, stat_out, stat_in, stat_m, final_out, final_in,
    loc_sem, ring_send, ring_recv, pair_send, pair_recv,
    tok_send, tok_recv, halo_send, halo_recv, par_send, par_recv,
    px_send, px_recv, st_send, st_recv, fin_send, fin_recv,
):
    n, tp, layers, ntaps, rows, width, chans, pieces = dims
    feats = width // tp
    drows = width // n
    ocols = width // n
    lch = chans // tp
    pch = 2 * lch
    half_rows = rows // 2
    reach = ntaps // 2
    grain = 16
    halo = grain * layers
    window = half_rows + 2 * halo
    main = half_rows + halo
    m = n // 2
    half_feats = width // 2

    sp = lax.axis_index("sp")
    t = lax.axis_index("tp")
    h = lax.rem(t, 2)
    xg = t // 2
    pair = t + 1 - 2 * h
    across = lax.rem(t + 2, tp)
    odd = lax.rem(sp, 2)
    pos = (1 - odd) * (sp // 2) + odd * (n - (sp + 1) // 2)

    def ring_sp(p):
        p = lax.rem(p + 2 * n, n)
        q = p // m
        return (1 - q) * (2 * p) + q * (2 * (n - p) - 1)

    right, left = ring_sp(pos + 1), ring_sp(pos - 1)
    up, down = lax.rem(sp + 1, n), lax.rem(sp + n - 1, n)

    barrier = pltpu.get_barrier_semaphore()
    has_up, has_down = 1 - (sp + 1) // n, 1 - (n - sp) // n
    has_halo = (1 - h) * has_down + h * has_up
    greet = [(sp, lax.rem(t + j, tp)) for j in range(1, tp)]
    greet += [(right, t), (left, t)]

    def block(layer, kind, origin, side, half=None):
        part, count = (0, 1) if half is None else (half, 2)
        if kind < 2:
            size = drows // count
            r = pl.ds(pl.multiple_of(origin * drows + part * size, size), size)
            return wvg.at[layer, side, kind, r, :]
        size = lch // count
        c = pl.ds(pl.multiple_of(origin * ocols, ocols), ocols)
        return wo.at[layer, pl.ds(pl.multiple_of(side * lch + part * size, size), size), c]

    def local_copy(layer, kind):
        src = (wv_in, wg_in, wo_in)[kind].at[layer]
        return pltpu.make_async_copy(src, block(layer, kind, sp, h), loc_sem.at[3 * layer + kind])

    def ring_copy(layer, kind, direction, step):
        shift = -(step - 1) if direction == 0 else step - 1
        half = direction if step == m else None
        ref = block(layer, kind, ring_sp(pos + shift), h, half)
        i = ((layer * 3 + kind) * 2 + direction) * m + step - 1
        return pltpu.make_async_remote_copy(
            src_ref=ref, dst_ref=ref, send_sem=ring_send.at[i], recv_sem=ring_recv.at[i],
            device_id=(right if direction == 0 else left, t), device_id_type=MESH)

    def ring_arrival(layer, kind, direction, step, side):
        shift = -step if direction == 0 else step
        half = direction if step == m else None
        return block(layer, kind, ring_sp(pos + shift), side, half)

    def pair_copy(layer, kind, direction, step, side):
        if step == 0:
            ref, j = block(layer, kind, sp, side), 0
        else:
            ref, j = ring_arrival(layer, kind, direction, step, side), direction * m + step
        i = (layer * 3 + kind) * (2 * m + 1) + j
        return pltpu.make_async_remote_copy(
            src_ref=ref, dst_ref=ref, send_sem=pair_send.at[i], recv_sem=pair_recv.at[i],
            device_id=(sp, pair), device_id_type=MESH)

    sequence = ring_order(layers, m)
    place = {e: i for i, e in enumerate(sequence)}
    sent, handled = [0], [0]

    def pump():
        while sent[0] < len(sequence):
            layer, kind, step = sequence[sent[0]]
            if step > 1 and place[layer, kind, step - 1] >= handled[0]:
                return
            if step == 1:
                local_copy(layer, kind).wait()
            for d in range(2):
                ring_copy(layer, kind, d, step).start()
            if step == 1:
                pair_copy(layer, kind, 0, 0, h).start()
            sent[0] += 1

    def advance(upto):
        while handled[0] < min(upto, len(sequence)):
            layer, kind, step = sequence[handled[0]]
            for d in range(2):
                ref = ring_arrival(layer, kind, d, step, h)
                i = ((layer * 3 + kind) * 2 + d) * m + step - 1
                pltpu.make_async_remote_copy(
                    src_ref=ref, dst_ref=ref, send_sem=ring_send.at[i], recv_sem=ring_recv.at[i],
                    device_id=(right, t), device_id_type=MESH).wait_recv()
            handled[0] += 1
            pump()
            for d in range(2):
                pair_copy(layer, kind, d, step, h).start()

    def advance_by(count):
        advance(handled[0] + count)

    def need(layer, *kinds):
        advance(max(place[layer, k, m] for k in kinds) + 1)
        for k in kinds:
            pair_copy(layer, k, 0, 0, 1 - h).wait_recv()
            for step in range(1, m + 1):
                for d in range(2):
                    pair_copy(layer, k, d, step, 1 - h).wait_recv()

    tcols = pl.ds(pl.multiple_of(t * feats, feats), feats)

    def window_cols(owner):
        return pl.ds(pl.multiple_of(owner * feats, feats), feats)

    def tok_copy(j):
        dest = lax.rem(t + j, tp)
        dh = lax.rem(dest, 2)
        return pltpu.make_async_remote_copy(
            src_ref=tok.at[pl.ds(pl.multiple_of(dh * (rows - main), grain), main), :],
            dst_ref=stream.at[pl.ds(pl.multiple_of((1 - dh) * halo, grain), main), tcols],
            send_sem=tok_send.at[j - 1], recv_sem=tok_recv.at[j - 1],
            device_id=(sp, dest), device_id_type=MESH)

    def tok_wait(j):
        owner = lax.rem(t + tp - j, tp)
        ref = stream.at[pl.ds(pl.multiple_of((1 - h) * halo, grain), main), window_cols(owner)]
        return pltpu.make_async_remote_copy(
            src_ref=ref, dst_ref=ref, send_sem=tok_send.at[j - 1], recv_sem=tok_recv.at[j - 1],
            device_id=(sp, pair), device_id_type=MESH)

    def greet_halo(there, row):
        @pl.when(there == 1)
        def _():
            for c in range(2):
                pl.semaphore_signal(barrier, inc=1, device_id=(row, 2 * xg + c), device_id_type=MESH)

    def halo_copy(side):
        src, row, there = ((rows - halo, 0, up), (0, main, down))[side]
        return pltpu.make_async_remote_copy(
            src_ref=tok.at[pl.ds(src, halo), :], dst_ref=stream.at[pl.ds(row, halo), tcols],
            send_sem=halo_send.at[side], recv_sem=halo_recv.at[t],
            device_id=(there, 2 * xg + side), device_id_type=MESH)

    def halo_pass(group, c):
        owner = 2 * group + c
        ref = stream.at[pl.ds(pl.multiple_of(h * main, grain), halo), window_cols(owner)]
        return pltpu.make_async_remote_copy(
            src_ref=ref, dst_ref=ref, send_sem=halo_send.at[2 + c], recv_sem=halo_recv.at[owner],
            device_id=(sp, across), device_id_type=MESH)

    def halo_start():
        for side, there in enumerate((has_up, has_down)):
            pl.when(there == 1)(lambda side=side: halo_copy(side).start())

    def halo_forward():
        @pl.when(has_halo == 1)
        def _():
            for c in range(2):
                halo_pass(xg, c).wait_recv()
                halo_pass(xg, c).start()

        @pl.when(has_halo == 0)
        def _():
            stream[pl.ds(pl.multiple_of(h * main, grain), halo), :] = jnp.zeros((halo, width), jnp.bfloat16)

    def halo_finish():
        @pl.when(has_halo == 1)
        def _():
            for c in range(2):
                halo_pass(1 - xg, c).wait_recv()
                halo_pass(xg, c).wait_send()

    def halo_sent():
        for side, there in enumerate((has_up, has_down)):
            pl.when(there == 1)(lambda side=side: halo_copy(side).wait_send())

    def param_copies():
        for i, (a, b) in enumerate(((taps_in, taps), (bias_in, bias), (lng_in, lng), (lns_in, lns))):
            yield pltpu.make_async_remote_copy(
                src_ref=a, dst_ref=b.at[h], send_sem=par_send.at[i], recv_sem=par_recv.at[i],
                device_id=(sp, pair), device_id_type=MESH)

    def param_waits():
        for i, (a, b) in enumerate(((taps_in, taps), (bias_in, bias), (lng_in, lng), (lns_in, lns))):
            yield pltpu.make_async_remote_copy(
                src_ref=a, dst_ref=b.at[1 - h], send_sem=par_send.at[i], recv_sem=par_recv.at[i],
                device_id=(sp, pair), device_id_type=MESH)

    for layer in range(layers):
        for kind in range(3):
            local_copy(layer, kind).start()
    for dev in greet:
        pl.semaphore_signal(barrier, inc=1, device_id=dev, device_id_type=MESH)
    greet_halo(has_up, up)
    greet_halo(has_down, down)
    pl.semaphore_wait(barrier, len(greet) + 2 * (has_up + has_down))

    pump()
    for j in range(1, tp):
        tok_copy(j).start()
    halo_start()
    for c in param_copies():
        c.start()

    stream[pl.ds(pl.multiple_of((1 - h) * halo, grain), main), tcols] = tok[
        pl.ds(pl.multiple_of(h * (rows - main), grain), main), :]
    taps[h] = taps_in[...]
    bias[h] = bias_in[...]
    lng[h] = lng_in[...]
    lns[h] = lns_in[...]
    stat_m[...] = jnp.zeros_like(stat_m)

    first_row = sp * rows + h * half_rows - halo
    total_rows = n * rows

    def project(layer, start, size):
        x = stream[pl.ds(start, size), :].astype(jnp.float32)
        scale = lax.rsqrt(jnp.mean(x * x, axis=-1, keepdims=True) + norm_floor)
        normed = (x * scale * gain_in[layer:layer + 1, :]).astype(jnp.bfloat16)
        row = lax.broadcasted_iota(jnp.int32, (size, lch), 0) + (first_row + start)
        inside = jnp.logical_and(row >= 0, row < total_rows)
        for c in range(2):
            value = jnp.dot(normed, wvg[layer, c, 0], preferred_element_type=jnp.float32)
            gate = jnp.dot(normed, wvg[layer, c, 1], preferred_element_type=jnp.float32)
            g = (value * jax.nn.sigmoid(gate)).astype(jnp.bfloat16).astype(jnp.float32)
            gated[pl.ds(start, size), c * lch:(c + 1) * lch] = jnp.where(inside, g, 0.0)

    def convolve(layer, start, r0, size):
        lanes_per = 128
        per_side = lch // lanes_per
        acc1[...] = jnp.zeros_like(acc1)
        acc2[...] = jnp.zeros_like(acc2)

        def lane_block(b, carry):
            c = b // per_side
            lane = pl.ds(pl.multiple_of(lax.rem(b, per_side) * lanes_per, lanes_per), lanes_per)
            wide = pl.ds(pl.multiple_of(b * lanes_per, lanes_per), lanes_per)
            total = jnp.zeros((size, lanes_per), jnp.float32) + bias[c, layer:layer + 1, lane]
            for k in range(ntaps):
                first = start + r0 + k - reach
                total = total + taps[c, layer, k:k + 1, lane] * gated[first:first + size, wide]
            conv[r0:r0 + size, wide] = total
            acc1[0:size, :] += total
            acc2[0:size, :] += total * total
            return carry

        lax.fori_loop(0, 2 * per_side, lane_block, 0)

    def send_stats(layer, i, size):
        lane_id = lax.broadcasted_iota(jnp.int32, (size, 128), 1)
        s1 = jnp.sum(acc1[0:size, :], axis=-1, keepdims=True)
        s2 = jnp.sum(acc2[0:size, :], axis=-1, keepdims=True)
        stat_m[0:size, :] = jnp.where(lane_id == 0, s1, jnp.where(lane_id == 1, s2, 0.0))
        stat_out[layer * pieces + i] = jnp.transpose(stat_m[...])[0:8, :]
        stat_copy(layer * pieces + i).start()

    def stat_copy(layer):
        return pltpu.make_async_remote_copy(
            src_ref=stat_out.at[layer], dst_ref=stat_in.at[layer], send_sem=st_send.at[layer],
            recv_sem=st_recv.at[layer], device_id=(sp, across), device_id_type=MESH)

    def part_copy(layer, i, r0, size, last):
        r = pl.ds(r0, size)
        if last:
            src = part_out.at[layer, r, pl.ds(pl.multiple_of((1 - xg) * half_feats, half_feats), half_feats)]
            dst = part_in.at[layer, r, pl.ds(pl.multiple_of((1 - xg) * half_feats, half_feats), half_feats)]
        else:
            src, dst = part_out.at[layer, r, :], part_in.at[layer, r, :]
        return pltpu.make_async_remote_copy(
            src_ref=src, dst_ref=dst, send_sem=px_send.at[layer * pieces + i],
            recv_sem=px_recv.at[layer * pieces + i], device_id=(sp, across), device_id_type=MESH)

    def finish_sends():
        halo_sent()
        for j in range(1, tp):
            tok_copy(j).wait_send()
        for c in param_copies():
            c.wait_send()
        for layer in range(layers):
            piece = (window - 2 * grain * (layer + 1)) // pieces
            for i in range(pieces):
                stat_copy(layer * pieces + i).wait_send()
                if layer < layers - 1:
                    part_copy(layer, i, i * piece, piece, False).wait_send()
            for kind in range(3):
                pair_copy(layer, kind, 0, 0, h).wait_send()
                for step in range(1, m + 1):
                    for d in range(2):
                        ring_copy(layer, kind, d, step).wait_send()
                        pair_copy(layer, kind, d, step, h).wait_send()

    advance(3)
    halo_forward()
    advance(max(place[0, 0, m], place[0, 1, m]) + 1)
    for j in range(1, tp):
        tok_wait(j).wait_recv()
    halo_finish()
    need(0, 0, 1)
    for i in range(2):
        project(0, i * (window // 2), window // 2)
    advance_by(1)
    for c in param_waits():
        c.wait_recv()

    for layer in range(layers):
        last = layer == layers - 1
        start = grain * (layer + 1)
        size = window - 2 * start
        piece = size // pieces
        for i in range(pieces):
            convolve(layer, start, i * piece, piece)
            send_stats(layer, i, piece)
            advance_by(1)
        need(layer, 2)
        for i in range(pieces):
            r0 = i * piece
            j = layer * pieces + i
            stat_copy(j).wait_recv()
            both = stat_out[j] + stat_in[j]
            wide = jnp.concatenate([both, jnp.zeros((120, both.shape[1]), jnp.float32)], axis=0)
            sums = jnp.transpose(wide)
            average = sums[0:piece, 0:1] / chans
            spread = sums[0:piece, 1:2] / chans - average * average
            scale = lax.rsqrt(spread + norm_floor)
            for c in range(2):
                y = (conv[r0:r0 + piece, c * lch:(c + 1) * lch] - average) * scale
                y = y * lng[c, layer:layer + 1, :] + lns[c, layer:layer + 1, :]
                act[r0:r0 + piece, c * lch:(c + 1) * lch] = (y / (1.0 + jnp.exp(-y))).astype(jnp.bfloat16)
            part_out[layer, r0:r0 + piece, :] = jnp.dot(
                act[r0:r0 + piece, :], wo[layer], preferred_element_type=jnp.float32).astype(jnp.bfloat16)
            part_copy(layer, i, r0, piece, last).start()
        if not last:
            need(layer + 1, 0, 1)
            for i in range(pieces):
                r0 = i * piece
                part_copy(layer, i, r0, piece, last).wait_recv()
                w0 = start + r0
                stream[w0:w0 + piece, :] = (
                    stream[w0:w0 + piece, :].astype(jnp.float32)
                    + part_out[layer, r0:r0 + piece, :].astype(jnp.float32)
                    + part_in[layer, r0:r0 + piece, :].astype(jnp.float32)).astype(jnp.bfloat16)
                project(layer + 1, w0, piece)
                advance_by(1)
        else:
            finish_sends()
            mycols = pl.ds(pl.multiple_of(xg * half_feats, half_feats), half_feats)

            def fin_copy(i, r0):
                return pltpu.make_async_remote_copy(
                    src_ref=final_out.at[pl.ds(r0, piece), pl.ds(pl.multiple_of((1 - h) * feats, feats), feats)],
                    dst_ref=final_in.at[pl.ds(r0, piece), :],
                    send_sem=fin_send.at[i], recv_sem=fin_recv.at[i],
                    device_id=(sp, pair), device_id_type=MESH)

            for i in range(pieces):
                r0 = i * piece
                ref = part_in.at[layer, pl.ds(r0, piece), mycols]
                pltpu.make_async_remote_copy(
                    src_ref=ref, dst_ref=ref, send_sem=px_send.at[layer * pieces + i],
                    recv_sem=px_recv.at[layer * pieces + i], device_id=(sp, across),
                    device_id_type=MESH).wait_recv()
                w0 = start + r0
                final_out[r0:r0 + piece, :] = (
                    stream[w0:w0 + piece, mycols].astype(jnp.float32)
                    + part_out[layer, r0:r0 + piece, mycols].astype(jnp.float32)
                    + part_in[layer, r0:r0 + piece, mycols].astype(jnp.float32)).astype(jnp.bfloat16)
                fin_copy(i, r0).start()
            out[pl.ds(pl.multiple_of(h * half_rows, grain), half_rows), :] = final_out[
                :, pl.ds(pl.multiple_of(h * feats, feats), feats)]
            for i in range(pieces):
                fin_copy(i, i * piece).wait_recv()
            out[pl.ds(pl.multiple_of((1 - h) * half_rows, grain), half_rows), :] = final_in[...]
            for i in range(pieces):
                fin_copy(i, i * piece).wait_send()
    for i in range(pieces):
        part_copy(layers - 1, i, i * (half_rows // pieces), half_rows // pieces, True).wait_send()


def fused_call(mesh, *args):
    tokens, norm_gain, w_value, w_gate, conv_taps, conv_bias, ln_gain, ln_shift, w_out = args
    n, tp = mesh.shape["sp"], mesh.shape["tp"]
    layers, ntaps, lch = conv_taps.shape
    rows, feats = tokens.shape
    width, chans = feats * tp, lch * tp
    pieces = 2
    half_rows = rows // 2
    window = half_rows + 32 * layers
    most = window - 32
    stat_rows = -(-most // pieces // 128) * 128
    m = n // 2
    dims = (n, tp, layers, ntaps, rows, width, chans, pieces)
    vmem = pl.BlockSpec(memory_space=pltpu.VMEM)
    anys = pl.BlockSpec(memory_space=pl.ANY)
    bf, f32 = jnp.bfloat16, jnp.float32
    dma = lambda k: pltpu.SemaphoreType.DMA((k,))
    ring_sems = layers * 3 * 2 * m
    pair_sems = layers * 3 * (2 * m + 1)
    return pl.pallas_call(
        functools.partial(fused, dims),
        out_shape=jax.ShapeDtypeStruct((rows, feats), bf),
        in_specs=[vmem, vmem, anys, anys, anys, vmem, vmem, vmem, vmem],
        out_specs=vmem,
        scratch_shapes=[
            pltpu.VMEM((layers, 2, 2, width, lch), bf),
            pltpu.VMEM((layers, 2 * lch, width), bf),
            pltpu.VMEM((2,) + conv_taps.shape, f32),
            pltpu.VMEM((2,) + conv_bias.shape, f32),
            pltpu.VMEM((2,) + ln_gain.shape, f32),
            pltpu.VMEM((2,) + ln_shift.shape, f32),
            pltpu.VMEM((window, width), bf),
            pltpu.VMEM((window, 2 * lch), f32),
            pltpu.VMEM((most, 2 * lch), f32),
            pltpu.VMEM((most // pieces, 128), f32),
            pltpu.VMEM((most // pieces, 128), f32),
            pltpu.VMEM((most, 2 * lch), bf),
            pltpu.VMEM((layers, most, width), bf),
            pltpu.VMEM((layers, most, width), bf),
            pltpu.VMEM((layers * pieces, 8, stat_rows), f32),
            pltpu.VMEM((layers * pieces, 8, stat_rows), f32),
            pltpu.VMEM((stat_rows, 128), f32),
            pltpu.VMEM((half_rows, 2 * feats), bf),
            pltpu.VMEM((half_rows, feats), bf),
            dma(3 * layers), dma(ring_sems), dma(ring_sems), dma(pair_sems), dma(pair_sems),
            dma(tp - 1), dma(tp - 1), dma(tp), dma(tp), dma(4), dma(4),
            dma(layers * pieces), dma(layers * pieces), dma(layers * pieces), dma(layers * pieces),
            dma(pieces), dma(pieces),
        ],
        compiler_params=pltpu.CompilerParams(
            collective_id=0, has_side_effects=True, vmem_limit_bytes=60 * 1024 * 1024),
    )(tokens, norm_gain, w_value, w_gate, w_out, conv_taps, conv_bias, ln_gain, ln_shift)


def fits(mesh, tokens, conv_taps, w_out):
    n, tp = mesh.shape["sp"], mesh.shape["tp"]
    layers, ntaps, lch = conv_taps.shape
    rows, feats = tokens.shape
    sizes = [rows // 2 + 32 * (layers - 1 - i) for i in range(layers)]
    return (tp == 4 and n % 2 == 0 and n >= 4 and ntaps % 2 == 1 and ntaps // 2 < 16
            and w_out.shape[2] % 128 == 0 and lch % 256 == 0 and feats % 128 == 0
            and rows % 32 == 0 and rows // 2 >= 16 * layers
            and all(s % 32 == 0 and s <= 256 for s in sizes)
            and layers * w_out.shape[1] * w_out.shape[2] * n * 12 <= 20 * 1024 * 1024)


def solution(mesh):
    placed = (
        P("sp", "tp"),
        P(),
        P(None, "sp", "tp"),
        P(None, "sp", "tp"),
        P(None, None, "tp"),
        P(None, "tp"),
        P(None, "tp"),
        P(None, "tp"),
        P(None, "tp", "sp"),
    )

    def run(*args):
        if fits(mesh, args[0], args[4], args[8]):
            return fused_call(mesh, *args)
        return body(*args)

    return jax.shard_map(run, mesh=mesh, in_specs=placed, out_specs=P("sp", "tp"), check_vma=False)
```

profile of v0, /device:TPU:0, one launch (start us, length us, event | category | flops | bytes accessed | tf_op | source)
XLA Modules:
  0.0 125.4 jit_solution(5265567282380650817)
XLA Ops:
  0.0 123.7 %shard_map.91 = bf16[384,512]{1,0:T(8,128)(2,1)} custom-call(bf16[384,512]{1,0:T(8,128)(2,1)} %tok.1, f32[3,2048]{1,0:T(4,128)} %gain_in.1, bf16[3,256,256]{2,1,0:T(8,128)(2,1)} %wv_in.1, bf16[3,256,256]{2,1,0:T(8,128)(2,1)} %wg_in.1, bf16[3,256,256]{2,1,0:T(8,128)(2,1)} %wo_in.1, f32[3,31,256]{2,1,0:T(8,128)} %taps_in.1, f32[3,256]{1,0:T(4,128)} %bias_in.1, ...), custom_call_target="tpu_custom_call" | custom-call | tf_op jit(solution)/shard_map/pallas_call | solution.py:515
  123.7 1.8 %copy.11 = bf16[384,512]{1,0:T(8,128)(2,1)} copy(bf16[384,512]{1,0:T(8,128)(2,1)} %shard_map.91) | data formatting | bytes 786432
where the time goes:
time: 126 us; the launch traced here: 125 us
  Pallas kernels  124 us (98%)
  local copies, waits for them, and re-layouts  1.77 us (1%)
    pallas_call x1, Pallas kernels, fused_call(): pl.pallas_call(functools.partial(fused, dims), out_shape=jax.ShapeDtypeSt...  124 us

commit v1 on v0

v1 whole, which is shorter than its diff:
```python
import functools

import jax
import jax.numpy as jnp
from jax import lax
from jax.experimental import pallas as pl
from jax.experimental.pallas import tpu as pltpu
from jax.sharding import PartitionSpec as P

MESH = pl.DeviceIdType.MESH

norm_floor = 0.01


def with_halo(array, sides, width):
    for axis, dim in sides:
        size, length = (lax.axis_size(axis), array.shape[dim])
        up = [(i, (i + 1) % size) for i in range(size - 1)]
        down = [(j, i) for i, j in up]
        last = lax.slice_in_dim(array, length - width, length, axis=dim)
        first = lax.slice_in_dim(array, 0, width, axis=dim)
        before = lax.ppermute(last, axis, up)
        after = lax.ppermute(first, axis, down)
        array = jnp.concatenate([before, array, after], axis=dim)
    return array


def body(tokens, norm_gain, w_value, w_gate, conv_taps, conv_bias, ln_gain, ln_shift, w_out):
    stream = tokens
    layer_count = w_value.shape[0]
    reach = conv_taps.shape[1] // 2
    local_channels = w_value.shape[2]
    channels = local_channels * lax.axis_size("tp")
    tok_rows = tokens.shape[0]
    whole_value, whole_gate = (
        lax.all_gather(w_value, "sp", axis=1, tiled=True),
        lax.all_gather(w_gate, "sp", axis=1, tiled=True),
    )
    whole_out = lax.all_gather(w_out, "sp", axis=2, tiled=True)
    for layer_index in range(layer_count):
        whole_rows = lax.all_gather(stream, "tp", axis=1, tiled=True)
        rows_f32 = whole_rows.astype(jnp.float32)
        scale_rows = lax.rsqrt(jnp.mean(rows_f32 * rows_f32, axis=-1, keepdims=True) + norm_floor)
        normed = (rows_f32 * scale_rows * norm_gain[layer_index]).astype(jnp.bfloat16)
        value_rows = jnp.dot(normed, whole_value[layer_index], preferred_element_type=jnp.float32)
        gate_rows = jnp.dot(normed, whole_gate[layer_index], preferred_element_type=jnp.float32)
        gated_input = (value_rows * jax.nn.sigmoid(gate_rows)).astype(jnp.bfloat16)
        padded = with_halo(gated_input, (("sp", 0),), reach)
        padded = padded.astype(jnp.float32)
        convolved = jnp.zeros((tok_rows, local_channels), jnp.float32) + conv_bias[layer_index]
        for offset in range(2 * reach + 1):
            convolved = (
                convolved + conv_taps[layer_index, offset] * padded[offset : offset + tok_rows]
            )
        moments = lax.psum(
            (
                jnp.sum(convolved, axis=-1, keepdims=True),
                jnp.sum(convolved * convolved, axis=-1, keepdims=True),
            ),
            "tp",
        )
        average = moments[0] / channels
        spread = moments[1] / channels - average * average
        activated = jax.nn.silu(
            (convolved - average) * lax.rsqrt(spread + norm_floor) * ln_gain[layer_index]
            + ln_shift[layer_index]
        ).astype(jnp.bfloat16)
        partial_rows = jnp.dot(
            activated, whole_out[layer_index], preferred_element_type=jnp.float32
        )
        summed = lax.psum_scatter(
            partial_rows.astype(jnp.bfloat16), "tp", scatter_dimension=1, tiled=True
        ).astype(jnp.float32)
        stream = (stream.astype(jnp.float32) + summed).astype(jnp.bfloat16)
    return stream


def fused(
    dims,
    tok, gain_in, wv_in, wg_in, wo_in, taps_in, bias_in, lng_in, lns_in,
    out,
    wvg, wo, taps, bias, lng, lns, stream, normed, gated, cv, cv2, act, resid,
    loc_sem, pre_send, pre_recv, z_send, z_recv, d_send, d_recv,
    a_send, a_recv, b_send, b_recv, r_send, r_recv, o_send, o_recv,
    tok_send, tok_recv, zh_send, zh_recv, hp_send, hp_recv, ih_send, ih_recv,
    par_send, par_recv, ln_send, ln_recv,
    ca_send, ca_recv, cb_send, cb_recv, cr_send, cr_recv,
    l_send, l_recv, p_send, p_recv, res_send, res_recv,
):
    n, tp, layers, ntaps, rows, width, chans = dims
    planes = n // 2
    feats = width // tp
    lch = chans // tp
    krows = width // n
    ocols = width // n
    reach = ntaps // 2
    grain = 16
    halo = grain * layers
    window = rows + 2 * halo
    slots = 2 * planes - 1
    last = layers - 1
    lanes = 128
    per_side = lch // lanes
    per_out = feats // ocols

    sp = lax.axis_index("sp")
    t = lax.axis_index("tp")
    z, y = sp // 2, lax.rem(sp, 2)
    x, h = t // 2, lax.rem(t, 2)
    xn, yn, hn = 1 - x, 1 - y, 1 - h
    same = 1 - (y + h - 2 * y * h)
    spn = 2 * z + yn
    has_up, has_down = 1 - (z + 1) // planes, jnp.minimum(z, 1)

    partner = (sp, 2 * x + hn)
    xdev = (sp, 2 * xn + h)
    ydev = (spn, t)
    ax, ay = hn * xn + h * x, hn * y + h * yn
    bx, by = hn * x + h * xn, hn * yn + h * y
    adev = (2 * z + ay, 2 * ax + h)
    bdev = (2 * z + by, 2 * bx + h)

    def rcopy(src, dst, ssem, rsem, dev):
        return pltpu.make_async_remote_copy(
            src_ref=src, dst_ref=dst, send_sem=ssem, recv_sem=rsem,
            device_id=dev, device_id_type=MESH)

    def arrived(ref, ssem, rsem):
        rcopy(ref, ref, ssem, rsem, partner).wait_recv()

    def when(flag):
        return pl.when(flag == 1)

    def vblock(l, k, zs, c):
        r = pl.ds(pl.multiple_of((2 * zs + c) * krows, krows), krows)
        return wvg.at[l, k, r, :]

    def oblock(l, zs, yy, cb):
        r = pl.ds(pl.multiple_of(cb * lch, lch), lch)
        return wo.at[l, 2 * zs + yy, r, :]

    def item(l, k, zs):
        return vblock(l, k, zs, h) if k < 2 else oblock(l, zs, y, t)

    def local_copy(l, k):
        src = (wv_in, wg_in, wo_in)[k].at[l]
        return pltpu.make_async_copy(src, item(l, k, z), loc_sem.at[3 * l + k])

    def pre_copy(l, k):
        src = (wv_in, wg_in)[k].at[l]
        i = 2 * l + k
        return rcopy(src, vblock(l, k, z, y), pre_send.at[i], pre_recv.at[i], (spn, 2 * x + hn))

    def z_copy(l, k, d, s):
        zs = z - s if d == 0 else z + s
        ref = item(l, k, zs)
        i = ((d * layers + l) * 3 + k) * (planes - 1) + s
        return rcopy(ref, ref, z_send.at[i], z_recv.at[i], (sp + (2 if d == 0 else -2), t))

    def z_wait(l, k, d, s):
        zs = z - s if d == 0 else z + s
        i = ((d * layers + l) * 3 + k) * (planes - 1) + s - 1
        arrived(item(l, k, zs), z_send.at[i], z_recv.at[i])

    def d_copy(l, k, src_kind, slot, ref):
        i = ((l * 3 + k) * slots + slot) if src_kind == 0 else (
            layers * 3 * slots + ((l * 3) + src_kind - 1) * slots + slot)
        return rcopy(ref, ref, d_send.at[i], d_recv.at[2 * l + k // 2], partner)

    def a_copy(l, slot, zs):
        ref, i = oblock(l, zs, y, t), l * slots + slot
        return rcopy(ref, ref, a_send.at[i], a_recv.at[i], adev)

    def b_copy(l, slot, zs):
        ref, i = oblock(l, zs, y, t), l * slots + slot
        return rcopy(ref, ref, b_send.at[i], b_recv.at[i], bdev)

    def r_copy(l, slot, zs):
        ref, i = oblock(l, zs, ay, 2 * ax + h), l * slots + slot
        return rcopy(ref, ref, r_send.at[i], r_recv.at[i], bdev)

    def o_copy(slot, rel, zs):
        ref, i = oblock(last, zs, y, t), 2 * slot + rel
        return rcopy(ref, ref, o_send.at[i], o_recv.at[2 * t + rel],
                     (sp if rel == 0 else spn, zs))

    def differs(a, b):
        return jnp.minimum(jnp.abs(a - b), 1)

    def spread(l, k, slot, zs):
        if k < 2:
            d_copy(l, k, 0, slot, item(l, k, zs)).start()
        elif l < last:
            a_copy(l, slot, zs).start()
            b_copy(l, slot, zs).start()
            d_copy(l, k, 0, slot, item(l, k, zs)).start()
        else:
            when(differs(zs, t))(lambda: o_copy(slot, 0, zs).start())
            o_copy(slot, 1, zs).start()

    def spread_sent(l, k, slot, zs):
        if k < 2:
            d_copy(l, k, 0, slot, item(l, k, zs)).wait_send()
        elif l < last:
            a_copy(l, slot, zs).wait_send()
            b_copy(l, slot, zs).wait_send()
            d_copy(l, k, 0, slot, item(l, k, zs)).wait_send()
        else:
            when(differs(zs, t))(lambda: o_copy(slot, 0, zs).wait_send())
            o_copy(slot, 1, zs).wait_send()

    def own_start(l, k):
        if k < 2:
            when(same)(lambda: local_copy(l, k).wait())

            @when(1 - same)
            def _():
                i = 2 * l + k
                arrived(item(l, k, z), pre_send.at[i], pre_recv.at[i])
        else:
            local_copy(l, k).wait()
        when(has_up)(lambda: z_copy(l, k, 0, 0).start())
        when(has_down)(lambda: z_copy(l, k, 1, 0).start())
        spread(l, k, 0, z)

    def below(s):
        return jnp.minimum(z // s, 1)

    def above(s):
        return jnp.minimum((planes - 1 - z) // s, 1)

    def groups(s):
        if s == 0:
            return [(None, 0, z)]
        return [(below(s), 2 * s - 1, z - s), (above(s), 2 * s, z + s)]

    def guarded(flag, f):
        if flag is None:
            f()
        else:
            when(flag)(f)

    def z_recv_step(l, k, s):
        for d, (flag, slot, zs) in enumerate(groups(s)):
            def go(d=d, slot=slot, zs=zs):
                z_wait(l, k, d, s)
                if s < planes - 1:
                    when((has_up, has_down)[d])(lambda: z_copy(l, k, d, s).start())
                spread(l, k, slot, zs)
            guarded(flag, go)

    def a_step(l, s):
        for flag, slot, zs in groups(s):
            def go(slot=slot, zs=zs):
                i = l * slots + slot
                ref = oblock(l, zs, ay, 2 * ax + h)
                arrived(ref, a_send.at[i], a_recv.at[i])
                r_copy(l, slot, zs).start()
                d_copy(l, 2, 1, slot, ref).start()
            guarded(flag, go)

    def b_step(l, s):
        for flag, slot, zs in groups(s):
            def go(slot=slot, zs=zs):
                i = l * slots + slot
                ref = oblock(l, zs, by, 2 * bx + h)
                arrived(ref, b_send.at[i], b_recv.at[i])
                d_copy(l, 2, 2, slot, ref).start()
            guarded(flag, go)

    def r_step(l, s):
        for flag, slot, zs in groups(s):
            def go(slot=slot, zs=zs):
                i = l * slots + slot
                ref = oblock(l, zs, yn, 2 * xn + h)
                arrived(ref, r_send.at[i], r_recv.at[i])
                d_copy(l, 2, 3, slot, ref).start()
            guarded(flag, go)

    def need_v(l):
        arrived(wvg.at[l, :, pl.ds(0, width // 2), :], d_send.at[0], d_recv.at[2 * l])

    def need_o(l):
        arrived(wo.at[l, pl.ds(0, planes)], d_send.at[0], d_recv.at[2 * l + 1])

    def need_last():
        for j in range(tp):
            other = lax.rem(t + j, tp)
            for rel in range(2):
                if j or rel:
                    i = 2 * other + rel
                    arrived(oblock(last, t, y if rel == 0 else yn, other), o_send.at[0], o_recv.at[i])

    def weights_sent():
        for l in range(layers):
            for k in range(3):
                if k < 2:
                    when(1 - same)(lambda l=l, k=k: pre_copy(l, k).wait_send())
                for s in range(planes - 1):
                    for d, flag in enumerate((has_up, has_down)):
                        ok = flag if s == 0 else flag * (below(s), above(s))[d]
                        when(ok)(lambda l=l, k=k, d=d, s=s: z_copy(l, k, d, s).wait_send())
                for s in range(planes):
                    for flag, slot, zs in groups(s):
                        guarded(flag, lambda l=l, k=k, slot=slot, zs=zs: spread_sent(l, k, slot, zs))

    def plane_sent():
        for l in range(last):
            for s in range(planes):
                for flag, slot, zs in groups(s):
                    def go(l=l, slot=slot, zs=zs):
                        r_copy(l, slot, zs).wait_send()
                        d_copy(l, 2, 1, slot, oblock(l, zs, ay, 2 * ax + h)).wait_send()
                        d_copy(l, 2, 2, slot, oblock(l, zs, by, 2 * bx + h)).wait_send()
                        d_copy(l, 2, 3, slot, oblock(l, zs, yn, 2 * xn + h)).wait_send()
                    guarded(flag, go)

    def cols(owner):
        return pl.ds(pl.multiple_of(owner * feats, feats), feats)

    def mcols(owner):
        return stream.at[pl.ds(halo, rows), cols(owner)]

    tcols = cols(t)

    def tok_copy(j):
        dev = ((sp, 2 * x + y), (sp, 2 * xn + y), (spn, 2 * x + y))[j]
        return rcopy(tok, mcols(t), tok_send.at[j], tok_recv.at[t], dev)

    rt = same * (2 * xn) + (1 - same) * (2 * x + 1)
    rsp = same * spn + (1 - same) * sp
    rtp = same * t + (1 - same) * (2 * xn + h)

    def tok_pass():
        return rcopy(mcols(rt), mcols(rt), tok_send.at[3], tok_recv.at[rt], (rsp, rtp))

    def tok_starts():
        when(1 - same)(lambda: tok_copy(0).start())
        tok_copy(1).start()
        tok_copy(2).start()

        @when(same)
        def _():
            stream[pl.ds(halo, rows), tcols] = tok[...]

    def tok_relay():
        arrived(mcols(rt), tok_send.at[3], tok_recv.at[rt])
        tok_pass().start()

    def tok_waits():
        for j in range(1, tp):
            other = lax.rem(rt + j, tp)
            ok = 1 - same * (1 - differs(other, t))
            when(ok)(lambda other=other: arrived(mcols(other), tok_send.at[3], tok_recv.at[other]))

    zh_to = y * has_up + yn * has_down
    zh_from = hn * has_down + h * has_up

    def edge(owner_cols, side):
        r = pl.ds(pl.multiple_of(side * (halo + rows), grain), halo)
        return stream.at[r, owner_cols]

    def zh_copy():
        src = tok.at[pl.ds(pl.multiple_of(y * (rows - halo), grain), halo), :]
        return rcopy(src, edge(tcols, yn), zh_send.at[0], zh_recv.at[t],
                     (sp + 4 * y - 2, 2 * x + yn))

    def half_cols(xx):
        return pl.ds(pl.multiple_of(xx * 2 * feats, feats), 2 * feats)

    def hp_copy(j):
        ref = edge(half_cols(xn if j == 2 else x), h)
        return rcopy(ref, ref, hp_send.at[j], hp_recv.at[j], xdev if j == 0 else ydev)

    def halo_pass():
        @when(zh_from * (1 - same))
        def _():
            for c in range(2):
                arrived(edge(cols(2 * x + c), h), zh_send.at[0], zh_recv.at[2 * x + c])
            hp_copy(0).start()
            hp_copy(1).start()

        @when(1 - zh_from)
        def _():
            stream[pl.ds(pl.multiple_of(h * (halo + rows), grain), halo), :] = jnp.zeros((halo, width), jnp.bfloat16)

    def halo_pass_on():
        @when(zh_from * (1 - same))
        def _():
            arrived(edge(half_cols(xn), h), hp_send.at[0], hp_recv.at[0])
            hp_copy(2).start()

    def halo_waits():
        @when(zh_from * same)
        def _():
            arrived(edge(half_cols(x), h), hp_send.at[0], hp_recv.at[1])
            arrived(edge(half_cols(xn), h), hp_send.at[0], hp_recv.at[2])

    def ih_copy():
        src = stream.at[pl.ds(pl.multiple_of(hn * rows + h * halo, grain), halo), :]
        dst = stream.at[pl.ds(pl.multiple_of(h * (halo + rows), grain), halo), :]
        return rcopy(src, dst, ih_send.at[0], ih_recv.at[0], partner)

    def ih_wait():
        ref = stream.at[pl.ds(pl.multiple_of(hn * (halo + rows), grain), halo), :]
        arrived(ref, ih_send.at[0], ih_recv.at[0])

    def par_copy(i):
        a, b = ((taps_in, taps), (bias_in, bias))[i]
        return rcopy(a, b, par_send.at[i], par_recv.at[i], partner)

    def ln_copy(i, j):
        a, b = ((lng_in, lng), (lns_in, lns))[i]
        return rcopy(a, b.at[t], ln_send.at[3 * i + j - 1], ln_recv.at[tp * i + t],
                     (sp, lax.rem(t + j, tp)))

    def params_start():
        for i in range(2):
            when(same)(lambda i=i: par_copy(i).start())
            for j in range(1, tp):
                ln_copy(i, j).start()

        @when(same)
        def _():
            taps[...] = taps_in[...]
            bias[...] = bias_in[...]
        lng[t] = lng_in[...]
        lns[t] = lns_in[...]

    def params_wait():
        for i, ref in enumerate((taps, bias)):
            when(1 - same)(lambda i=i, ref=ref: arrived(ref, par_send.at[i], par_recv.at[i]))
        for i, ref in enumerate((lng, lns)):
            for j in range(1, tp):
                other = lax.rem(t + j, tp)
                arrived(ref.at[other], ln_send.at[0], ln_recv.at[tp * i + other])

    def small_sent():
        when(1 - same)(lambda: tok_copy(0).wait_send())
        tok_copy(1).wait_send()
        tok_copy(2).wait_send()
        when(zh_to)(lambda: zh_copy().wait_send())
        for i in range(2):
            when(same)(lambda i=i: par_copy(i).wait_send())
            for j in range(1, tp):
                ln_copy(i, j).wait_send()

    def stream_sent():
        tok_pass().wait_send()

        @when(zh_from * (1 - same))
        def _():
            for j in range(3):
                hp_copy(j).wait_send()
        ih_copy().wait_send()

    cb_own = 2 * x + y
    cb_a, cb_b, cb_d = 2 * ax + ay, 2 * bx + by, 2 * xn + yn

    def piece(l, i):
        size = (window - 2 * grain * (l + 1)) // 2
        return i * size, size

    def cblock(l, i, cb):
        r0, size = piece(l, i)
        return cv.at[l, cb, pl.ds(r0, size), :]

    def cv_copy(l, i, j):
        ref = cblock(l, i, cb_a if j == 2 else cb_own)
        s, r = ((ca_send, ca_recv), (cb_send, cb_recv), (cr_send, cr_recv))[j]
        return rcopy(ref, ref, s.at[2 * l + i], r.at[2 * l + i], adev if j == 0 else bdev)

    def cv_start(l, i):
        cv_copy(l, i, 0).start()
        cv_copy(l, i, 1).start()

    def cv_relay(l, i):
        arrived(cblock(l, i, cb_a), ca_send.at[2 * l + i], ca_recv.at[2 * l + i])
        cv_copy(l, i, 2).start()

    def cv_waits(l, i):
        arrived(cblock(l, i, cb_b), cb_send.at[2 * l + i], cb_recv.at[2 * l + i])
        arrived(cblock(l, i, cb_d), cr_send.at[2 * l + i], cr_recv.at[2 * l + i])

    def lblock(i, cb):
        r0, size = piece(last, i)
        return cv2.at[cb, pl.ds(r0, size), :]

    def l_copy(i, j):
        src, cb, dev = (
            (cblock(last, i, cb_own), cb_own, ydev),
            (cblock(last, i, cb_own), cb_own, xdev),
            (lblock(i, 2 * x + yn), 2 * x + yn, xdev),
        )[j]
        return rcopy(src, lblock(i, cb), l_send.at[3 * i + j], l_recv.at[3 * i + j], dev)

    def p_copy(i, j):
        cb = (cb_own, 2 * x + yn, 2 * xn + y, 2 * xn + yn)[j]
        src = cblock(last, i, cb) if j == 0 else lblock(i, cb)
        return rcopy(src, lblock(i, cb), p_send.at[tp * i + j], p_recv.at[tp * i + j], partner)

    def last_start(i):
        r0, size = piece(last, i)
        when(1 - same)(lambda: l_copy(i, 0).start())

        @when(same)
        def _():
            l_copy(i, 1).start()
            p_copy(i, 0).start()
            cv2[cb_own, r0:r0 + size, :] = cv[last, cb_own, r0:r0 + size, :]

    def last_relay(i):
        @when(same)
        def _():
            arrived(lblock(i, 2 * x + yn), l_send.at[0], l_recv.at[3 * i])
            l_copy(i, 2).start()
            p_copy(i, 1).start()

    def last_waits(i):
        @when(same)
        def _():
            for j in (1, 2):
                cb = 2 * xn + (y if j == 1 else yn)
                arrived(lblock(i, cb), l_send.at[0], l_recv.at[3 * i + j])
                p_copy(i, j + 1).start()

        @when(1 - same)
        def _():
            for j, cb in enumerate((2 * x + yn, 2 * x + y, 2 * xn + yn, 2 * xn + y)):
                arrived(lblock(i, cb), p_send.at[0], p_recv.at[tp * i + j])

    def conv_sent():
        for i in range(2):
            for l in range(last):
                for j in range(3):
                    cv_copy(l, i, j).wait_send()
            when(1 - same)(lambda i=i: l_copy(i, 0).wait_send())

            @when(same)
            def _(i=i):
                l_copy(i, 1).wait_send()
                l_copy(i, 2).wait_send()
                for j in range(tp):
                    p_copy(i, j).wait_send()

    def res_copy():
        src = stream.at[pl.ds(halo, rows), cols(2 * x + hn)]
        return rcopy(src, resid, res_send.at[0], res_recv.at[0], partner)

    def res_start():
        @when(same)
        def _():
            res_copy().start()
            resid[...] = stream[pl.ds(halo, rows), tcols]

    def res_wait():
        when(1 - same)(lambda: arrived(resid, res_send.at[0], res_recv.at[0]))

    first_row = (2 * z + h) * rows - halo
    total_rows = n * rows

    def normalize(layer, w0, size):
        def step(i, carry):
            r = pl.ds(pl.multiple_of(w0 + i * grain, grain), grain)
            v = stream[r, :].astype(jnp.float32)
            scale = lax.rsqrt(jnp.mean(v * v, axis=-1, keepdims=True) + norm_floor)
            normed[r, :] = (v * scale * gain_in[layer:layer + 1, :]).astype(jnp.bfloat16)
            return carry

        lax.fori_loop(0, size // grain, step, 0)

    def project(layer, w0, size):
        value = jnp.dot(normed[w0:w0 + size, :], wvg[layer, 0], preferred_element_type=jnp.float32)
        gate = jnp.dot(normed[w0:w0 + size, :], wvg[layer, 1], preferred_element_type=jnp.float32)
        g = (value * jax.nn.sigmoid(gate)).astype(jnp.bfloat16).astype(jnp.float32)
        row = lax.broadcasted_iota(jnp.int32, (size, lch), 0) + (first_row + w0)
        g = jnp.where(jnp.logical_and(row >= 0, row < total_rows), g, 0.0)
        for b in range(per_side):
            gated[b, w0:w0 + size, :] = g[:, b * lanes:(b + 1) * lanes]

    def convolve(layer, i):
        r0, size = piece(layer, i)
        start = grain * (layer + 1)
        cut = -(-size // 2 // grain) * grain
        for c0, part in ((r0, cut), (r0 + cut, size - cut)):
            def lane_block(b, carry, c0=c0, part=part):
                lane = pl.ds(pl.multiple_of(b * lanes, lanes), lanes)
                total = jnp.zeros((part, lanes), jnp.float32) + bias[layer:layer + 1, lane]
                for k in range(ntaps):
                    first = start + c0 + k - reach
                    total = total + taps[layer, k:k + 1, lane] * gated[b, first:first + part, :]
                cv[layer, cb_own, c0:c0 + part, lane] = total.astype(jnp.bfloat16)
                return carry

            lax.fori_loop(0, per_side, lane_block, 0)

    def activate(layer, i):
        r0, size = piece(layer, i)

        def step(j, carry):
            r = pl.ds(pl.multiple_of(r0 + j * grain, grain), grain)
            src = [(cv[layer, b, r, :] if layer < last else cv2[b, r, :]).astype(jnp.float32) for b in range(tp)]
            s1 = sum(jnp.sum(v, axis=-1, keepdims=True) for v in src)
            s2 = sum(jnp.sum(v * v, axis=-1, keepdims=True) for v in src)
            average = s1 / chans
            spread_ = s2 / chans - average * average
            scale = lax.rsqrt(spread_ + norm_floor)
            for b, v in enumerate(src):
                u = (v - average) * scale * lng[b, layer:layer + 1, :] + lns[b, layer:layer + 1, :]
                act[r, b * lch:(b + 1) * lch] = (u / (1.0 + jnp.exp(-u))).astype(jnp.bfloat16)
            return carry

        lax.fori_loop(0, size // grain, step, 0)

    def expand(layer, i):
        r0, size = piece(layer, i)
        w0 = grain * (layer + 1) + r0

        def step(j, carry):
            c = pl.ds(pl.multiple_of(j * ocols, ocols), ocols)
            add = jnp.dot(act[r0:r0 + size, :], wo[layer, j], preferred_element_type=jnp.float32)
            stream[w0:w0 + size, c] = (stream[w0:w0 + size, c].astype(jnp.float32) + add).astype(jnp.bfloat16)
            return carry

        lax.fori_loop(0, n, step, 0)

    def finish(i):
        r0, size = piece(last, i)
        for j in range(per_out):
            c = slice(j * ocols, (j + 1) * ocols)
            add = jnp.dot(act[r0:r0 + size, :], wo[last, per_out * t + j], preferred_element_type=jnp.float32)
            out[r0:r0 + size, c] = (resid[r0:r0 + size, c].astype(jnp.float32) + add).astype(jnp.bfloat16)

    barrier = pltpu.get_barrier_semaphore()
    for l in range(layers):
        for k in range(3):
            if k < 2:
                when(same)(lambda l=l, k=k: local_copy(l, k).start())
            else:
                local_copy(l, k).start()
    for ds in range(2):
        for j in range(tp):
            if ds or j:
                pl.semaphore_signal(barrier, inc=1, device_id=((sp, spn)[ds], lax.rem(t + j, tp)), device_id_type=MESH)
    for flag, step in ((has_up, 2), (has_down, -2)):
        @when(flag)
        def _(step=step):
            for c in range(2):
                pl.semaphore_signal(barrier, inc=1, device_id=(sp + step, 2 * x + c), device_id_type=MESH)
    pl.semaphore_wait(barrier, 2 * tp - 1 + 2 * (has_up + has_down))

    def pre_start(l):
        for k in range(2):
            when(1 - same)(lambda k=k: pre_copy(l, k).start())

    pre_start(0)
    when(zh_to)(lambda: zh_copy().start())
    tok_starts()
    params_start()
    own_start(0, 0)
    own_start(0, 1)
    pre_start(1)
    pre_start(2)
    z_recv_step(0, 0, 1)
    z_recv_step(0, 1, 1)
    halo_pass()
    tok_relay()
    halo_pass_on()
    z_recv_step(0, 0, 2)
    z_recv_step(0, 1, 2)
    own_start(0, 2)
    tok_waits()
    ih_copy().start()
    halo_waits()
    ih_wait()
    normalize(0, 0, window)
    params_wait()
    z_recv_step(0, 0, 3)
    z_recv_step(0, 1, 3)
    need_v(0)

    for layer in range(layers):
        w0 = grain * layer
        half = (window - 2 * w0) // 2
        for i in range(2):
            project(layer, w0 + i * half, half)
        if layer < last:
            own_start(layer + 1, 0)
            own_start(layer + 1, 1)
            for i in range(2):
                convolve(layer, i)
                cv_start(layer, i)
            z_recv_step(layer, 2, 1)
            a_step(layer, 0)
            cv_relay(layer, 0)
            cv_relay(layer, 1)
            z_recv_step(layer, 2, 2)
            a_step(layer, 1)
            b_step(layer, 0)
            z_recv_step(layer, 2, 3)
            z_recv_step(layer + 1, 0, 1)
            z_recv_step(layer + 1, 1, 1)
            for i in range(2):
                cv_waits(layer, i)
                activate(layer, i)
            a_step(layer, 2)
            b_step(layer, 1)
            r_step(layer, 0)
            z_recv_step(layer + 1, 0, 2)
            z_recv_step(layer + 1, 1, 2)
            own_start(layer + 1, 2)
            a_step(layer, 3)
            b_step(layer, 2)
            r_step(layer, 1)
            b_step(layer, 3)
            r_step(layer, 2)
            r_step(layer, 3)
            need_o(layer)
            if layer == 0:
                stream_sent()
            for i in range(2):
                expand(layer, i)
            if layer + 1 == last:
                res_start()
            normalize(layer + 1, grain * (layer + 1), window - 2 * grain * (layer + 1))
            z_recv_step(layer + 1, 0, 3)
            z_recv_step(layer + 1, 1, 3)
            need_v(layer + 1)
        else:
            z_recv_step(last, 2, 1)
            for i in range(2):
                convolve(last, i)
                last_start(i)
            for i in range(2):
                last_relay(i)
            z_recv_step(last, 2, 2)
            for i in range(2):
                last_waits(i)
            z_recv_step(last, 2, 3)
            res_wait()
            for i in range(2):
                activate(last, i)
            need_last()
            for i in range(2):
                finish(i)
    weights_sent()
    plane_sent()
    small_sent()
    conv_sent()
    when(same)(lambda: res_copy().wait_send())


def fused_call(mesh, *args):
    tokens, norm_gain, w_value, w_gate, conv_taps, conv_bias, ln_gain, ln_shift, w_out = args
    n, tp = mesh.shape["sp"], mesh.shape["tp"]
    layers, ntaps, lch = conv_taps.shape
    rows, feats = tokens.shape
    width, chans = feats * tp, lch * tp
    planes = n // 2
    slots = 2 * planes - 1
    halo = 16 * layers
    window = rows + 2 * halo
    most = window - 32
    dims = (n, tp, layers, ntaps, rows, width, chans)
    vmem = pl.BlockSpec(memory_space=pltpu.VMEM)
    anys = pl.BlockSpec(memory_space=pl.ANY)
    bf, f32 = jnp.bfloat16, jnp.float32
    dma = lambda k: pltpu.SemaphoreType.DMA((k,))
    pairs = lambda k: [dma(k), dma(k)]
    wide = (layers - 1) * slots
    return pl.pallas_call(
        functools.partial(fused, dims),
        out_shape=jax.ShapeDtypeStruct((rows, feats), bf),
        in_specs=[vmem, vmem, anys, anys, anys, vmem, vmem, vmem, vmem],
        out_specs=vmem,
        scratch_shapes=[
            pltpu.VMEM((layers, 2, width, lch), bf),
            pltpu.VMEM((layers, n, chans, width // n), bf),
            pltpu.VMEM(conv_taps.shape, f32),
            pltpu.VMEM(conv_bias.shape, f32),
            pltpu.VMEM((tp,) + ln_gain.shape, f32),
            pltpu.VMEM((tp,) + ln_shift.shape, f32),
            pltpu.VMEM((window, width), bf),
            pltpu.VMEM((window, width), bf),
            pltpu.VMEM((lch // 128, window, 128), f32),
            pltpu.VMEM((layers, tp, most, lch), bf),
            pltpu.VMEM((tp, rows, lch), bf),
            pltpu.VMEM((most, chans), bf),
            pltpu.VMEM((rows, feats), bf),
            dma(3 * layers),
            *pairs(2 * layers),
            *pairs(2 * layers * 3 * (planes - 1)),
            dma(layers * 3 * slots * 2), dma(2 * layers),
            *pairs(wide), *pairs(wide), *pairs(wide),
            *pairs(2 * slots),
            *pairs(tp), *pairs(tp), *pairs(3), *pairs(1),
            *pairs(2), dma(6), dma(2 * tp),
            *pairs(2 * layers), *pairs(2 * layers), *pairs(2 * layers),
            *pairs(6), *pairs(2 * tp), *pairs(1),
        ],
        compiler_params=pltpu.CompilerParams(
            collective_id=0, has_side_effects=True, vmem_limit_bytes=60 * 1024 * 1024),
    )(tokens, norm_gain, w_value, w_gate, w_out, conv_taps, conv_bias, ln_gain, ln_shift)


def fits(mesh, tokens, conv_taps, w_out):
    n, tp = mesh.shape["sp"], mesh.shape["tp"]
    layers, ntaps, lch = conv_taps.shape
    rows, feats = tokens.shape
    return (tp == 4 and n == 2 * tp and ntaps % 2 == 1 and ntaps // 2 < 16 and layers > 1
            and w_out.shape[2] % 128 == 0 and lch % 128 == 0 and feats % 128 == 0
            and feats == 2 * w_out.shape[2]
            and rows % 32 == 0 and rows >= 32 * layers and rows <= 512
            and layers * w_out.shape[1] * w_out.shape[2] * n * 12 <= 20 * 1024 * 1024)


def solution(mesh):
    placed = (
        P("sp", "tp"),
        P(),
        P(None, "sp", "tp"),
        P(None, "sp", "tp"),
        P(None, None, "tp"),
        P(None, "tp"),
        P(None, "tp"),
        P(None, "tp"),
        P(None, "tp", "sp"),
    )

    def run(*args):
        if fits(mesh, args[0], args[4], args[8]):
            return fused_call(mesh, *args)
        return body(*args)

    return jax.shard_map(run, mesh=mesh, in_specs=placed, out_specs=P("sp", "tp"), check_vma=False)
```

time: 126 us -> 141 us (1.12)
  Pallas kernels: 124 us -> 138 us
    pallas_call x1, Pallas kernels: 124 us -> 138 us  [fused_call(): pl.pallas_call(functools.partial(fused, dims), out_shape=jax.ShapeDtypeSt...]
where the time goes in v1:
time: 141 us; the launch traced here: 140 us
  Pallas kernels  138 us (98%)
  local copies, waits for them, and re-layouts  1.77 us (1%)
    pallas_call x1, Pallas kernels, fused_call(): pl.pallas_call(functools.partial(fused, dims), out_shape=jax.ShapeDtypeSt...  138 us

profile of v1, /device:TPU:0, one launch (start us, length us, event | category | flops | bytes accessed | tf_op | source)
XLA Modules:
  0.0 139.6 jit_solution(11964045679951704459)
XLA Ops:
  0.0 137.8 %shard_map.91 = bf16[384,512]{1,0:T(8,128)(2,1)} custom-call(bf16[384,512]{1,0:T(8,128)(2,1)} %tok.1, f32[3,2048]{1,0:T(4,128)} %gain_in.1, bf16[3,256,256]{2,1,0:T(8,128)(2,1)} %wv_in.1, bf16[3,256,256]{2,1,0:T(8,128)(2,1)} %wg_in.1, bf16[3,256,256]{2,1,0:T(8,128)(2,1)} %wo_in.1, f32[3,31,256]{2,1,0:T(8,128)} %taps_in.1, f32[3,256]{1,0:T(4,128)} %bias_in.1, ...), custom_call_target="tpu_custom_call" | custom-call | tf_op jit(solution)/shard_map/pallas_call | solution.py:771
  137.8 1.8 %copy.11 = bf16[384,512]{1,0:T(8,128)(2,1)} copy(bf16[384,512]{1,0:T(8,128)(2,1)} %shard_map.91) | data formatting | bytes 786432

commit v2 on v1

--- a/solution.py
+++ b/solution.py
@@ -79,7 +79,7 @@
     dims,
     tok, gain_in, wv_in, wg_in, wo_in, taps_in, bias_in, lng_in, lns_in,
     out,
-    wvg, wo, taps, bias, lng, lns, stream, normed, gated, cv, cv2, act, resid,
+    wvg, wo, taps, bias, lng, lns, stream, normed, gated, cv, cv2, act, resid, rowa, rowb,
     loc_sem, pre_send, pre_recv, z_send, z_recv, d_send, d_recv,
     a_send, a_recv, b_send, b_recv, r_send, r_recv, o_send, o_recv,
     tok_send, tok_recv, zh_send, zh_recv, hp_send, hp_recv, ih_send, ih_recv,
@@ -102,6 +102,7 @@
     lanes = 128
     per_side = lch // lanes
     per_out = feats // ocols
+    swapped = 1
 
     sp = lax.axis_index("sp")
     t = lax.axis_index("tp")
@@ -120,6 +121,11 @@
     adev = (2 * z + ay, 2 * ax + h)
     bdev = (2 * z + by, 2 * bx + h)
 
+    def route(slot):
+        if (slot + 1) // 2 < swapped:
+            return (x, yn), ydev, (xn, y), xdev
+        return (ax, ay), adev, (bx, by), bdev
+
     def rcopy(src, dst, ssem, rsem, dev):
         return pltpu.make_async_remote_copy(
             src_ref=src, dst_ref=dst, send_sem=ssem, recv_sem=rsem,
@@ -165,19 +171,27 @@
     def d_copy(l, k, src_kind, slot, ref):
         i = ((l * 3 + k) * slots + slot) if src_kind == 0 else (
             layers * 3 * slots + ((l * 3) + src_kind - 1) * slots + slot)
-        return rcopy(ref, ref, d_send.at[i], d_recv.at[2 * l + k // 2], partner)
+        return rcopy(ref, ref, d_send.at[i], d_recv.at[l if k < 2 else layers + l * slots + slot], partner)
 
     def a_copy(l, slot, zs):
         ref, i = oblock(l, zs, y, t), l * slots + slot
-        return rcopy(ref, ref, a_send.at[i], a_recv.at[i], adev)
+        return rcopy(ref, ref, a_send.at[i], a_recv.at[i], route(slot)[1])
 
     def b_copy(l, slot, zs):
         ref, i = oblock(l, zs, y, t), l * slots + slot
-        return rcopy(ref, ref, b_send.at[i], b_recv.at[i], bdev)
+        return rcopy(ref, ref, b_send.at[i], b_recv.at[i], route(slot)[3])
+
+    def from_a(l, slot, zs):
+        px, py = route(slot)[0]
+        return oblock(l, zs, py, 2 * px + h)
+
+    def from_b(l, slot, zs):
+        px, py = route(slot)[2]
+        return oblock(l, zs, py, 2 * px + h)
 
     def r_copy(l, slot, zs):
-        ref, i = oblock(l, zs, ay, 2 * ax + h), l * slots + slot
-        return rcopy(ref, ref, r_send.at[i], r_recv.at[i], bdev)
+        ref, i = from_a(l, slot, zs), l * slots + slot
+        return rcopy(ref, ref, r_send.at[i], r_recv.at[i], route(slot)[3])
 
     def o_copy(slot, rel, zs):
         ref, i = oblock(last, zs, y, t), 2 * slot + rel
@@ -187,16 +201,20 @@
     def differs(a, b):
         return jnp.minimum(jnp.abs(a - b), 1)
 
-    def spread(l, k, slot, zs):
-        if k < 2:
+    def to_partner(l, k, slot, zs):
+        if k < 2 or l < last:
             d_copy(l, k, 0, slot, item(l, k, zs)).start()
-        elif l < last:
-            a_copy(l, slot, zs).start()
-            b_copy(l, slot, zs).start()
-            d_copy(l, k, 0, slot, item(l, k, zs)).start()
-        else:
-            when(differs(zs, t))(lambda: o_copy(slot, 0, zs).start())
-            o_copy(slot, 1, zs).start()
+
+    def spread(l, s):
+        for flag, slot, zs in groups(s):
+            def go(slot=slot, zs=zs):
+                if l < last:
+                    a_copy(l, slot, zs).start()
+                    b_copy(l, slot, zs).start()
+                else:
+                    when(differs(zs, t))(lambda: o_copy(slot, 0, zs).start())
+                    o_copy(slot, 1, zs).start()
+            guarded(flag, go)
 
     def spread_sent(l, k, slot, zs):
         if k < 2:
@@ -221,7 +239,7 @@
             local_copy(l, k).wait()
         when(has_up)(lambda: z_copy(l, k, 0, 0).start())
         when(has_down)(lambda: z_copy(l, k, 1, 0).start())
-        spread(l, k, 0, z)
+        to_partner(l, k, 0, z)
 
     def below(s):
         return jnp.minimum(z // s, 1)
@@ -246,14 +264,14 @@
                 z_wait(l, k, d, s)
                 if s < planes - 1:
                     when((has_up, has_down)[d])(lambda: z_copy(l, k, d, s).start())
-                spread(l, k, slot, zs)
+                to_partner(l, k, slot, zs)
             guarded(flag, go)
 
     def a_step(l, s):
         for flag, slot, zs in groups(s):
             def go(slot=slot, zs=zs):
                 i = l * slots + slot
-                ref = oblock(l, zs, ay, 2 * ax + h)
+                ref = from_a(l, slot, zs)
                 arrived(ref, a_send.at[i], a_recv.at[i])
                 r_copy(l, slot, zs).start()
                 d_copy(l, 2, 1, slot, ref).start()
@@ -263,7 +281,7 @@
         for flag, slot, zs in groups(s):
             def go(slot=slot, zs=zs):
                 i = l * slots + slot
-                ref = oblock(l, zs, by, 2 * bx + h)
+                ref = from_b(l, slot, zs)
                 arrived(ref, b_send.at[i], b_recv.at[i])
                 d_copy(l, 2, 2, slot, ref).start()
             guarded(flag, go)
@@ -278,10 +296,7 @@
             guarded(flag, go)
 
     def need_v(l):
-        arrived(wvg.at[l, :, pl.ds(0, width // 2), :], d_send.at[0], d_recv.at[2 * l])
-
-    def need_o(l):
-        arrived(wo.at[l, pl.ds(0, planes)], d_send.at[0], d_recv.at[2 * l + 1])
+        arrived(wvg.at[l, :, pl.ds(0, width // 2), :], d_send.at[0], d_recv.at[l])
 
     def need_last():
         for j in range(tp):
@@ -310,8 +325,8 @@
                 for flag, slot, zs in groups(s):
                     def go(l=l, slot=slot, zs=zs):
                         r_copy(l, slot, zs).wait_send()
-                        d_copy(l, 2, 1, slot, oblock(l, zs, ay, 2 * ax + h)).wait_send()
-                        d_copy(l, 2, 2, slot, oblock(l, zs, by, 2 * bx + h)).wait_send()
+                        d_copy(l, 2, 1, slot, from_a(l, slot, zs)).wait_send()
+                        d_copy(l, 2, 2, slot, from_b(l, slot, zs)).wait_send()
                         d_copy(l, 2, 3, slot, oblock(l, zs, yn, 2 * xn + h)).wait_send()
                     guarded(flag, go)
 
@@ -327,31 +342,59 @@
         dev = ((sp, 2 * x + y), (sp, 2 * xn + y), (spn, 2 * x + y))[j]
         return rcopy(tok, mcols(t), tok_send.at[j], tok_recv.at[t], dev)
 
-    rt = same * (2 * xn) + (1 - same) * (2 * x + 1)
-    rsp = same * spn + (1 - same) * sp
-    rtp = same * t + (1 - same) * (2 * xn + h)
-
-    def tok_pass():
-        return rcopy(mcols(rt), mcols(rt), tok_send.at[3], tok_recv.at[rt], (rsp, rtp))
+    half_rows = rows // 2
+
+    def hcols(owner, part):
+        return stream.at[pl.ds(halo + part * half_rows, half_rows), cols(owner)]
+
+    def tok_pass(j):
+        if j == 0:
+            ref, i, dev, k = hcols(2 * xn + yn, 0), 2 * xn + yn, ydev, 3
+        elif j == 1:
+            ref, i, dev, k = mcols(2 * x + yn), 2 * x + yn, xdev, 3
+        else:
+            ref, i, dev, k = hcols(2 * x + y, 1), tp, xdev, 4
+        return rcopy(ref, ref, tok_send.at[k], tok_recv.at[i], dev)
 
     def tok_starts():
         when(1 - same)(lambda: tok_copy(0).start())
         tok_copy(1).start()
-        tok_copy(2).start()
 
         @when(same)
         def _():
             stream[pl.ds(halo, rows), tcols] = tok[...]
 
+    def tok_arrived(ref, i):
+        arrived(ref, tok_send.at[3], tok_recv.at[i])
+
     def tok_relay():
-        arrived(mcols(rt), tok_send.at[3], tok_recv.at[rt])
-        tok_pass().start()
+        @when(same)
+        def _():
+            tok_arrived(mcols(2 * xn + yn), 2 * xn + yn)
+            tok_pass(0).start()
+
+        @when(1 - same)
+        def _():
+            tok_arrived(mcols(2 * x + yn), 2 * x + yn)
+            tok_pass(1).start()
+
+    def tok_relay_late():
+        @when(1 - same)
+        def _():
+            tok_arrived(mcols(2 * x + y), 2 * x + y)
+            tok_pass(2).start()
 
     def tok_waits():
-        for j in range(1, tp):
-            other = lax.rem(rt + j, tp)
-            ok = 1 - same * (1 - differs(other, t))
-            when(ok)(lambda other=other: arrived(mcols(other), tok_send.at[3], tok_recv.at[other]))
+        @when(same)
+        def _():
+            tok_arrived(mcols(2 * x + hn), 2 * x + hn)
+            tok_arrived(mcols(2 * xn + y), 2 * xn + y)
+
+        @when(1 - same)
+        def _():
+            tok_arrived(mcols(2 * xn + yn), 2 * xn + yn)
+            tok_arrived(hcols(2 * xn + y, 0), 2 * xn + y)
+            tok_arrived(hcols(2 * xn + y, 1), tp)
 
     zh_to = y * has_up + yn * has_down
     zh_from = hn * has_down + h * has_up
@@ -446,7 +489,12 @@
                 ln_copy(i, j).wait_send()
 
     def stream_sent():
-        tok_pass().wait_send()
+        when(same)(lambda: tok_pass(0).wait_send())
+
+        @when(1 - same)
+        def _():
+            tok_pass(1).wait_send()
+            tok_pass(2).wait_send()
 
         @when(zh_from * (1 - same))
         def _():
@@ -458,8 +506,9 @@
     cb_a, cb_b, cb_d = 2 * ax + ay, 2 * bx + by, 2 * xn + yn
 
     def piece(l, i):
-        size = (window - 2 * grain * (l + 1)) // 2
-        return i * size, size
+        total = window - 2 * grain * (l + 1)
+        first = total - rows // 2
+        return i * first, total - first if i else first
 
     def cblock(l, i, cb):
         r0, size = piece(l, i)
@@ -559,20 +608,45 @@
     first_row = (2 * z + h) * rows - halo
     total_rows = n * rows
 
-    def normalize(layer, w0, size):
+    def over_rows(start, size, block, f):
         def step(i, carry):
-            r = pl.ds(pl.multiple_of(w0 + i * grain, grain), grain)
-            v = stream[r, :].astype(jnp.float32)
-            scale = lax.rsqrt(jnp.mean(v * v, axis=-1, keepdims=True) + norm_floor)
-            normed[r, :] = (v * scale * gain_in[layer:layer + 1, :]).astype(jnp.bfloat16)
+            f(pl.ds(pl.multiple_of(start + i * block, grain), block))
             return carry
 
-        lax.fori_loop(0, size // grain, step, 0)
-
-    def project(layer, w0, size):
+        lax.fori_loop(0, size // block, step, 0)
+
+    def chunk(layer, i):
+        r0, size = piece(layer - 1, i)
+        return grain * layer + r0, size
+
+    def normalize(layer, i):
+        w0, size = chunk(layer, i)
+        block = 2 * grain
+
+        def squares(r):
+            total = jnp.zeros((block, lanes), jnp.float32)
+            for c in range(width // lanes):
+                v = stream[r, c * lanes:(c + 1) * lanes].astype(jnp.float32)
+                total = total + v * v
+            rowa[r, :] = total
+
+        def scaled(r):
+            scale = rowa[r, :]
+            for c in range(width // lanes):
+                lane = slice(c * lanes, (c + 1) * lanes)
+                v = stream[r, lane].astype(jnp.float32)
+                normed[r, lane] = (v * scale * gain_in[layer:layer + 1, lane]).astype(jnp.bfloat16)
+
+        over_rows(w0, size, block, squares)
+        mean = jnp.sum(rowa[w0:w0 + size, :], axis=-1, keepdims=True) / width
+        rowa[w0:w0 + size, :] = jnp.broadcast_to(lax.rsqrt(mean + norm_floor), (size, lanes))
+        over_rows(w0, size, block, scaled)
+
+    def project(layer, i):
+        w0, size = chunk(layer, i)
         value = jnp.dot(normed[w0:w0 + size, :], wvg[layer, 0], preferred_element_type=jnp.float32)
         gate = jnp.dot(normed[w0:w0 + size, :], wvg[layer, 1], preferred_element_type=jnp.float32)
-        g = (value * jax.nn.sigmoid(gate)).astype(jnp.bfloat16).astype(jnp.float32)
+        g = (value * (0.5 + 0.5 * jnp.tanh(0.5 * gate))).astype(jnp.bfloat16).astype(jnp.float32)
         row = lax.broadcasted_iota(jnp.int32, (size, lch), 0) + (first_row + w0)
         g = jnp.where(jnp.logical_and(row >= 0, row < total_rows), g, 0.0)
         for b in range(per_side):
@@ -596,33 +670,58 @@
 
     def activate(layer, i):
         r0, size = piece(layer, i)
-
-        def step(j, carry):
-            r = pl.ds(pl.multiple_of(r0 + j * grain, grain), grain)
-            src = [(cv[layer, b, r, :] if layer < last else cv2[b, r, :]).astype(jnp.float32) for b in range(tp)]
-            s1 = sum(jnp.sum(v, axis=-1, keepdims=True) for v in src)
-            s2 = sum(jnp.sum(v * v, axis=-1, keepdims=True) for v in src)
-            average = s1 / chans
-            spread_ = s2 / chans - average * average
-            scale = lax.rsqrt(spread_ + norm_floor)
-            for b, v in enumerate(src):
-                u = (v - average) * scale * lng[b, layer:layer + 1, :] + lns[b, layer:layer + 1, :]
-                act[r, b * lch:(b + 1) * lch] = (u / (1.0 + jnp.exp(-u))).astype(jnp.bfloat16)
-            return carry
-
-        lax.fori_loop(0, size // grain, step, 0)
-
-    def expand(layer, i):
-        r0, size = piece(layer, i)
-        w0 = grain * (layer + 1) + r0
-
-        def step(j, carry):
-            c = pl.ds(pl.multiple_of(j * ocols, ocols), ocols)
-            add = jnp.dot(act[r0:r0 + size, :], wo[layer, j], preferred_element_type=jnp.float32)
-            stream[w0:w0 + size, c] = (stream[w0:w0 + size, c].astype(jnp.float32) + add).astype(jnp.bfloat16)
-            return carry
-
-        lax.fori_loop(0, n, step, 0)
+        block = 2 * grain if size % (2 * grain) == 0 else grain
+        parts = [(b, c) for b in range(tp) for c in range(per_side)]
+
+        def load(b, c, r):
+            lane = slice(c * lanes, (c + 1) * lanes)
+            return (cv[layer, b, r, lane] if layer < last else cv2[b, r, lane]).astype(jnp.float32)
+
+        def sums(r):
+            s1 = jnp.zeros((block, lanes), jnp.float32)
+            s2 = jnp.zeros((block, lanes), jnp.float32)
+            for b, c in parts:
+                v = load(b, c, r)
+                s1 = s1 + v
+                s2 = s2 + v * v
+            rowa[r, :] = s1
+            rowb[r, :] = s2
+
+        def apply(r):
+            scale, shift = rowa[r, :], rowb[r, :]
+            for b, c in parts:
+                lane = slice(c * lanes, (c + 1) * lanes)
+                u = (load(b, c, r) - shift) * scale
+                u = 0.5 * (u * lng[b, layer:layer + 1, lane] + lns[b, layer:layer + 1, lane])
+                act[r, b * lch + c * lanes:b * lch + (c + 1) * lanes] = (u + u * jnp.tanh(u)).astype(jnp.bfloat16)
+
+        over_rows(r0, size, block, sums)
+        rows_ = slice(r0, r0 + size)
+        average = jnp.sum(rowa[rows_, :], axis=-1, keepdims=True) / chans
+        spread_ = jnp.sum(rowb[rows_, :], axis=-1, keepdims=True) / chans - average * average
+        rowa[rows_, :] = jnp.broadcast_to(lax.rsqrt(spread_ + norm_floor), (size, lanes))
+        rowb[rows_, :] = jnp.broadcast_to(average, (size, lanes))
+        over_rows(r0, size, block, apply)
+
+    def expand_wait(layer, s):
+        for flag, slot, zs in groups(s):
+            sem = d_recv.at[layers + layer * slots + slot]
+            guarded(flag, lambda sem=sem: arrived(wo.at[layer, 0], d_send.at[0], sem))
+
+    def expand(layer, s, pieces=(0, 1)):
+        for flag, slot, zs in groups(s):
+            def go(slot=slot, zs=zs):
+                def step(j, carry):
+                    c = pl.ds(pl.multiple_of((2 * zs + j) * ocols, ocols), ocols)
+                    for i in pieces:
+                        r0, size = piece(layer, i)
+                        w0 = grain * (layer + 1) + r0
+                        add = jnp.dot(act[r0:r0 + size, :], wo[layer, 2 * zs + j], preferred_element_type=jnp.float32)
+                        stream[w0:w0 + size, c] = (stream[w0:w0 + size, c].astype(jnp.float32) + add).astype(jnp.bfloat16)
+                    return carry
+
+                lax.fori_loop(0, 2, step, 0)
+            guarded(flag, go)
 
     def finish(i):
         r0, size = piece(last, i)
@@ -656,93 +755,114 @@
     pre_start(0)
     when(zh_to)(lambda: zh_copy().start())
     tok_starts()
+    halo_pass()
+    tok_copy(2).start()
     params_start()
     own_start(0, 0)
     own_start(0, 1)
-    pre_start(1)
-    pre_start(2)
     z_recv_step(0, 0, 1)
+    tok_relay()
     z_recv_step(0, 1, 1)
-    halo_pass()
-    tok_relay()
+    own_start(0, 2)
     halo_pass_on()
     z_recv_step(0, 0, 2)
+    tok_relay_late()
+    pre_start(1)
     z_recv_step(0, 1, 2)
-    own_start(0, 2)
+    spread(0, 0)
+    z_recv_step(0, 2, 1)
     tok_waits()
     ih_copy().start()
     halo_waits()
     ih_wait()
-    normalize(0, 0, window)
+    normalize(0, 0)
+    normalize(0, 1)
     params_wait()
     z_recv_step(0, 0, 3)
     z_recv_step(0, 1, 3)
+    own_start(1, 0)
+    own_start(1, 1)
+    spread(0, 1)
     need_v(0)
-
-    for layer in range(layers):
-        w0 = grain * layer
-        half = (window - 2 * w0) // 2
+    for i in range(2):
+        project(0, i)
+        convolve(0, i)
+        cv_start(0, i)
+        if i == 0:
+            a_step(0, 0)
+            z_recv_step(0, 2, 2)
+    pre_start(2)
+
+    for layer in range(last):
+        after = layer + 1
+        cv_relay(layer, 0)
+        cv_relay(layer, 1)
+        spread(layer, 2)
+        z_recv_step(layer, 2, 3)
+        spread(layer, 3)
+        z_recv_step(after, 0, 1)
+        b_step(layer, 0)
+        a_step(layer, 1)
+        z_recv_step(after, 1, 1)
         for i in range(2):
-            project(layer, w0 + i * half, half)
-        if layer < last:
-            own_start(layer + 1, 0)
-            own_start(layer + 1, 1)
-            for i in range(2):
-                convolve(layer, i)
-                cv_start(layer, i)
-            z_recv_step(layer, 2, 1)
-            a_step(layer, 0)
-            cv_relay(layer, 0)
-            cv_relay(layer, 1)
-            z_recv_step(layer, 2, 2)
-            a_step(layer, 1)
-            b_step(layer, 0)
-            z_recv_step(layer, 2, 3)
-            z_recv_step(layer + 1, 0, 1)
-            z_recv_step(layer + 1, 1, 1)
-            for i in range(2):
-                cv_waits(layer, i)
-                activate(layer, i)
-            a_step(layer, 2)
-            b_step(layer, 1)
-            r_step(layer, 0)
-            z_recv_step(layer + 1, 0, 2)
-            z_recv_step(layer + 1, 1, 2)
-            own_start(layer + 1, 2)
-            a_step(layer, 3)
-            b_step(layer, 2)
-            r_step(layer, 1)
-            b_step(layer, 3)
-            r_step(layer, 2)
-            r_step(layer, 3)
-            need_o(layer)
-            if layer == 0:
-                stream_sent()
-            for i in range(2):
-                expand(layer, i)
-            if layer + 1 == last:
-                res_start()
-            normalize(layer + 1, grain * (layer + 1), window - 2 * grain * (layer + 1))
-            z_recv_step(layer + 1, 0, 3)
-            z_recv_step(layer + 1, 1, 3)
-            need_v(layer + 1)
-        else:
-            z_recv_step(last, 2, 1)
-            for i in range(2):
-                convolve(last, i)
+            cv_waits(layer, i)
+            activate(layer, i)
+        z_recv_step(after, 0, 2)
+        r_step(layer, 0)
+        a_step(layer, 2)
+        z_recv_step(after, 1, 2)
+        own_start(after, 2)
+        if layer == 0:
+            stream_sent()
+        expand_wait(layer, 0)
+        expand(layer, 0)
+        b_step(layer, 1)
+        a_step(layer, 3)
+        r_step(layer, 1)
+        spread(after, 0)
+        z_recv_step(after, 0, 3)
+        expand_wait(layer, 1)
+        expand(layer, 1)
+        b_step(layer, 2)
+        z_recv_step(after, 1, 3)
+        if after < last:
+            own_start(after + 1, 0)
+            own_start(after + 1, 1)
+        r_step(layer, 2)
+        expand_wait(layer, 2)
+        expand(layer, 2)
+        b_step(layer, 3)
+        need_v(after)
+        r_step(layer, 3)
+        z_recv_step(after, 2, 1)
+        spread(after, 1)
+        expand_wait(layer, 3)
+        for i in range(2):
+            expand(layer, 3, (i,))
+            normalize(after, i)
+            project(after, i)
+            convolve(after, i)
+            if after < last:
+                cv_start(after, i)
+                if i == 0:
+                    a_step(after, 0)
+            else:
                 last_start(i)
-            for i in range(2):
-                last_relay(i)
-            z_recv_step(last, 2, 2)
-            for i in range(2):
-                last_waits(i)
-            z_recv_step(last, 2, 3)
-            res_wait()
-            for i in range(2):
-                activate(last, i)
-            need_last()
-            for i in range(2):
-                finish(i)
+        z_recv_step(after, 2, 2)
+    res_start()
+    last_relay(0)
+    last_relay(1)
+    spread(last, 2)
+    z_recv_step(last, 2, 3)
+    spread(last, 3)
+    res_wait()
+    last_waits(0)
+    activate(last, 0)
+    last_waits(1)
+    activate(last, 1)
+    need_last()
+    finish(0)
+    finish(1)
     weights_sent()
     plane_sent()
     small_sent()
@@ -787,13 +907,15 @@
             pltpu.VMEM((tp, rows, lch), bf),
             pltpu.VMEM((most, chans), bf),
             pltpu.VMEM((rows, feats), bf),
+            pltpu.VMEM((window, 128), f32),
+            pltpu.VMEM((window, 128), f32),
             dma(3 * layers),
             *pairs(2 * layers),
             *pairs(2 * layers * 3 * (planes - 1)),
-            dma(layers * 3 * slots * 2), dma(2 * layers),
+            dma(layers * 3 * slots * 2), dma(layers * (1 + slots)),
             *pairs(wide), *pairs(wide), *pairs(wide),
             *pairs(2 * slots),
-            *pairs(tp), *pairs(tp), *pairs(3), *pairs(1),
+            *pairs(tp + 1), *pairs(tp), *pairs(3), *pairs(1),
             *pairs(2), dma(6), dma(2 * tp),
             *pairs(2 * layers), *pairs(2 * layers), *pairs(2 * layers),
             *pairs(6), *pairs(2 * tp), *pairs(1),
@@ -810,7 +932,7 @@
     return (tp == 4 and n == 2 * tp and ntaps % 2 == 1 and ntaps // 2 < 16 and layers > 1
             and w_out.shape[2] % 128 == 0 and lch % 128 == 0 and feats % 128 == 0
             and feats == 2 * w_out.shape[2]
-            and rows % 32 == 0 and rows >= 32 * layers and rows <= 512
+            and rows % 64 == 0 and rows >= 32 * layers and rows <= 512
             and layers * w_out.shape[1] * w_out.shape[2] * n * 12 <= 20 * 1024 * 1024)
 
 

time: 141 us -> 117 us (0.83)
  Pallas kernels: 138 us -> 115 us
    pallas_call x1, Pallas kernels: 138 us -> 115 us  [fused_call(): pl.pallas_call(functools.partial(fused, dims), out_shape=jax.ShapeDtypeSt...]
where the time goes in v2:
time: 117 us
  Pallas kernels  115 us (98%)
  local copies, waits for them, and re-layouts  1.77 us (2%)
    pallas_call x1, Pallas kernels, fused_call(): pl.pallas_call(functools.partial(fused, dims), out_shape=jax.ShapeDtypeSt...  115 us

profile of v2, /device:TPU:0, one launch (start us, length us, event | category | flops | bytes accessed | tf_op | source)
XLA Modules:
  0.0 116.8 jit_solution(15704090819933082588)
XLA Ops:
  0.0 115.0 %shard_map.91 = bf16[384,512]{1,0:T(8,128)(2,1)} custom-call(bf16[384,512]{1,0:T(8,128)(2,1)} %tok.1, f32[3,2048]{1,0:T(4,128)} %gain_in.1, bf16[3,256,256]{2,1,0:T(8,128)(2,1)} %wv_in.1, bf16[3,256,256]{2,1,0:T(8,128)(2,1)} %wg_in.1, bf16[3,256,256]{2,1,0:T(8,128)(2,1)} %wo_in.1, f32[3,31,256]{2,1,0:T(8,128)} %taps_in.1, f32[3,256]{1,0:T(4,128)} %bias_in.1, ...), custom_call_target="tpu_custom_call" | custom-call | tf_op jit(solution)/shard_map/pallas_call | solution.py:891
  115.0 1.8 %copy.11 = bf16[384,512]{1,0:T(8,128)(2,1)} copy(bf16[384,512]{1,0:T(8,128)(2,1)} %shard_map.91) | data formatting | bytes 786432

commit v3 on v2

--- a/solution.py
+++ b/solution.py
@@ -77,11 +77,11 @@
 
 def fused(
     dims,
-    tok, gain_in, wv_in, wg_in, wo_in, taps_in, bias_in, lng_in, lns_in,
+    tok_in, gain_hbm, wv_in, wg_in, wo_in, taps_in, bias_in, lng_in, lns_in,
     out,
-    wvg, wo, taps, bias, lng, lns, stream, normed, gated, cv, cv2, act, resid, rowa, rowb,
-    loc_sem, pre_send, pre_recv, z_send, z_recv, d_send, d_recv,
-    a_send, a_recv, b_send, b_recv, r_send, r_recv, o_send, o_recv,
+    tok, gain_in, result, wvg, wo, taps, bias, lng, lns, stream, normed, gated, cv, cv2, act, resid, rowa, rowb,
+    loc_sem, in_sem, out_sem, pre_send, pre_recv, z_send, z_recv, d_send, d_recv,
+    a_send, a_recv, b_send, b_recv, r_send, r_recv, o_send, o_recv, op_send,
     tok_send, tok_recv, zh_send, zh_recv, hp_send, hp_recv, ih_send, ih_recv,
     par_send, par_recv, ln_send, ln_recv,
     ca_send, ca_recv, cb_send, cb_recv, cr_send, cr_recv,
@@ -121,9 +121,11 @@
     adev = (2 * z + ay, 2 * ax + h)
     bdev = (2 * z + by, 2 * bx + h)
 
-    def route(slot):
+    def route(l, slot):
         if (slot + 1) // 2 < swapped:
-            return (x, yn), ydev, (xn, y), xdev
+            if l == 0:
+                return (x, yn), ydev, (xn, y), xdev
+            return (xn, y), xdev, (x, yn), ydev
         return (ax, ay), adev, (bx, by), bdev
 
     def rcopy(src, dst, ssem, rsem, dev):
@@ -175,23 +177,23 @@
 
     def a_copy(l, slot, zs):
         ref, i = oblock(l, zs, y, t), l * slots + slot
-        return rcopy(ref, ref, a_send.at[i], a_recv.at[i], route(slot)[1])
+        return rcopy(ref, ref, a_send.at[i], a_recv.at[i], route(l, slot)[1])
 
     def b_copy(l, slot, zs):
         ref, i = oblock(l, zs, y, t), l * slots + slot
-        return rcopy(ref, ref, b_send.at[i], b_recv.at[i], route(slot)[3])
+        return rcopy(ref, ref, b_send.at[i], b_recv.at[i], route(l, slot)[3])
 
     def from_a(l, slot, zs):
-        px, py = route(slot)[0]
+        px, py = route(l, slot)[0]
         return oblock(l, zs, py, 2 * px + h)
 
     def from_b(l, slot, zs):
-        px, py = route(slot)[2]
+        px, py = route(l, slot)[2]
         return oblock(l, zs, py, 2 * px + h)
 
     def r_copy(l, slot, zs):
         ref, i = from_a(l, slot, zs), l * slots + slot
-        return rcopy(ref, ref, r_send.at[i], r_recv.at[i], route(slot)[3])
+        return rcopy(ref, ref, r_send.at[i], r_recv.at[i], route(l, slot)[3])
 
     def o_copy(slot, rel, zs):
         ref, i = oblock(last, zs, y, t), 2 * slot + rel
@@ -213,8 +215,21 @@
                     b_copy(l, slot, zs).start()
                 else:
                     when(differs(zs, t))(lambda: o_copy(slot, 0, zs).start())
-                    o_copy(slot, 1, zs).start()
+                    when(1 - differs(zs // 2, x))(lambda: o_copy(slot, 1, zs).start())
             guarded(flag, go)
+
+    def o_pass(c):
+        owner = 2 * xn + c
+        ref = oblock(last, t, y, owner)
+        return rcopy(ref, ref, op_send.at[c], o_recv.at[2 * owner + 1], ydev)
+
+    def o_relay(s):
+        @when(1 - differs(jnp.abs(z - t), s))
+        def _():
+            for c in range(2):
+                owner = 2 * xn + c
+                arrived(oblock(last, t, y, owner), o_send.at[0], o_recv.at[2 * owner])
+                o_pass(c).start()
 
     def spread_sent(l, k, slot, zs):
         if k < 2:
@@ -225,7 +240,7 @@
             d_copy(l, k, 0, slot, item(l, k, zs)).wait_send()
         else:
             when(differs(zs, t))(lambda: o_copy(slot, 0, zs).wait_send())
-            o_copy(slot, 1, zs).wait_send()
+            when(1 - differs(zs // 2, x))(lambda: o_copy(slot, 1, zs).wait_send())
 
     def own_start(l, k):
         if k < 2:
@@ -299,12 +314,11 @@
         arrived(wvg.at[l, :, pl.ds(0, width // 2), :], d_send.at[0], d_recv.at[l])
 
     def need_last():
+        mate = 2 * x + hn
+        arrived(oblock(last, t, y, mate), o_send.at[0], o_recv.at[2 * mate])
         for j in range(tp):
             other = lax.rem(t + j, tp)
-            for rel in range(2):
-                if j or rel:
-                    i = 2 * other + rel
-                    arrived(oblock(last, t, y if rel == 0 else yn, other), o_send.at[0], o_recv.at[i])
+            arrived(oblock(last, t, yn, other), o_send.at[0], o_recv.at[2 * other + 1])
 
     def weights_sent():
         for l in range(layers):
@@ -320,6 +334,8 @@
                         guarded(flag, lambda l=l, k=k, slot=slot, zs=zs: spread_sent(l, k, slot, zs))
 
     def plane_sent():
+        for c in range(2):
+            o_pass(c).wait_send()
         for l in range(last):
             for s in range(planes):
                 for flag, slot, zs in groups(s):
@@ -333,68 +349,73 @@
     def cols(owner):
         return pl.ds(pl.multiple_of(owner * feats, feats), feats)
 
-    def mcols(owner):
-        return stream.at[pl.ds(halo, rows), cols(owner)]
-
     tcols = cols(t)
-
-    def tok_copy(j):
-        dev = ((sp, 2 * x + y), (sp, 2 * xn + y), (spn, 2 * x + y))[j]
-        return rcopy(tok, mcols(t), tok_send.at[j], tok_recv.at[t], dev)
 
     half_rows = rows // 2
 
     def hcols(owner, part):
         return stream.at[pl.ds(halo + part * half_rows, half_rows), cols(owner)]
 
+    def tok_copy(j, p):
+        dev = ((sp, 2 * x + y), (sp, 2 * xn + y), (spn, 2 * x + y))[j]
+        return rcopy(tok.at[pl.ds(p * half_rows, half_rows), :], hcols(t, p),
+                     tok_send.at[2 * j + p], tok_recv.at[2 * t + p], dev)
+
+    def tok_start(j):
+        tok_copy(j, 0).start()
+        tok_copy(j, 1).start()
+
     def tok_pass(j):
-        if j == 0:
-            ref, i, dev, k = hcols(2 * xn + yn, 0), 2 * xn + yn, ydev, 3
-        elif j == 1:
-            ref, i, dev, k = mcols(2 * x + yn), 2 * x + yn, xdev, 3
-        else:
-            ref, i, dev, k = hcols(2 * x + y, 1), tp, xdev, 4
-        return rcopy(ref, ref, tok_send.at[k], tok_recv.at[i], dev)
+        owner, p, dev = (
+            (2 * xn + yn, 0, ydev), (2 * x + yn, 0, xdev),
+            (2 * x + yn, 1, xdev), (2 * x + y, 1, xdev))[j]
+        ref = hcols(owner, p)
+        return rcopy(ref, ref, tok_send.at[6 + j], tok_recv.at[2 * owner + p], dev)
 
     def tok_starts():
-        when(1 - same)(lambda: tok_copy(0).start())
-        tok_copy(1).start()
+        when(1 - same)(lambda: tok_start(0))
+        tok_start(1)
 
         @when(same)
         def _():
             stream[pl.ds(halo, rows), tcols] = tok[...]
 
-    def tok_arrived(ref, i):
-        arrived(ref, tok_send.at[3], tok_recv.at[i])
-
-    def tok_relay():
+    def tok_arrived(owner, p):
+        arrived(hcols(owner, p), tok_send.at[0], tok_recv.at[2 * owner + p])
+
+    def tok_relay(step):
         @when(same)
         def _():
-            tok_arrived(mcols(2 * xn + yn), 2 * xn + yn)
-            tok_pass(0).start()
+            if step == 0:
+                tok_arrived(2 * xn + yn, 0)
+                tok_pass(0).start()
 
         @when(1 - same)
         def _():
-            tok_arrived(mcols(2 * x + yn), 2 * x + yn)
-            tok_pass(1).start()
-
-    def tok_relay_late():
-        @when(1 - same)
-        def _():
-            tok_arrived(mcols(2 * x + y), 2 * x + y)
-            tok_pass(2).start()
+            if step == 0:
+                tok_arrived(2 * x + yn, 0)
+                tok_pass(1).start()
+            elif step == 1:
+                tok_arrived(2 * x + yn, 1)
+                tok_pass(2).start()
+            else:
+                tok_arrived(2 * x + y, 1)
+                tok_pass(3).start()
 
     def tok_waits():
         @when(same)
         def _():
-            tok_arrived(mcols(2 * x + hn), 2 * x + hn)
-            tok_arrived(mcols(2 * xn + y), 2 * xn + y)
+            tok_arrived(2 * xn + yn, 1)
+            for p in range(2):
+                tok_arrived(2 * x + hn, p)
+                tok_arrived(2 * xn + y, p)
 
         @when(1 - same)
         def _():
-            tok_arrived(mcols(2 * xn + yn), 2 * xn + yn)
-            tok_arrived(hcols(2 * xn + y, 0), 2 * xn + y)
-            tok_arrived(hcols(2 * xn + y, 1), tp)
+            tok_arrived(2 * x + y, 0)
+            for p in range(2):
+                tok_arrived(2 * xn + yn, p)
+                tok_arrived(2 * xn + y, p)
 
     zh_to = y * has_up + yn * has_down
     zh_from = hn * has_down + h * has_up
@@ -463,14 +484,33 @@
             for j in range(1, tp):
                 ln_copy(i, j).start()
 
-        @when(same)
-        def _():
-            taps[...] = taps_in[...]
-            bias[...] = bias_in[...]
-        lng[t] = lng_in[...]
-        lns[t] = lns_in[...]
+
+    def in_copies():
+        return [
+            pltpu.make_async_copy(a, b, in_sem.at[i])
+            for i, (a, b) in enumerate((
+                (tok_in, tok), (gain_hbm, gain_in), (lng_in, lng.at[t]), (lns_in, lns.at[t]),
+                (taps_in, taps), (bias_in, bias)))
+        ]
+
+    def in_start():
+        for i, c in enumerate(in_copies()):
+            if i < 4:
+                c.start()
+            else:
+                when(same)(lambda c=c: c.start())
+
+    def out_copy(i):
+        r0, size = piece(last, i)
+        r = pl.ds(r0, size)
+        return pltpu.make_async_copy(result.at[r, :], out.at[r, :], out_sem.at[i])
 
     def params_wait():
+        for i, c in enumerate(in_copies()):
+            if i >= 4:
+                when(same)(lambda c=c: c.wait())
+            elif i > 0:
+                c.wait()
         for i, ref in enumerate((taps, bias)):
             when(1 - same)(lambda i=i, ref=ref: arrived(ref, par_send.at[i], par_recv.at[i]))
         for i, ref in enumerate((lng, lns)):
@@ -479,9 +519,10 @@
                 arrived(ref.at[other], ln_send.at[0], ln_recv.at[tp * i + other])
 
     def small_sent():
-        when(1 - same)(lambda: tok_copy(0).wait_send())
-        tok_copy(1).wait_send()
-        tok_copy(2).wait_send()
+        for p in range(2):
+            when(1 - same)(lambda p=p: tok_copy(0, p).wait_send())
+            tok_copy(1, p).wait_send()
+            tok_copy(2, p).wait_send()
         when(zh_to)(lambda: zh_copy().wait_send())
         for i in range(2):
             when(same)(lambda i=i: par_copy(i).wait_send())
@@ -493,8 +534,8 @@
 
         @when(1 - same)
         def _():
-            tok_pass(1).wait_send()
-            tok_pass(2).wait_send()
+            for j in range(1, 4):
+                tok_pass(j).wait_send()
 
         @when(zh_from * (1 - same))
         def _():
@@ -728,9 +769,10 @@
         for j in range(per_out):
             c = slice(j * ocols, (j + 1) * ocols)
             add = jnp.dot(act[r0:r0 + size, :], wo[last, per_out * t + j], preferred_element_type=jnp.float32)
-            out[r0:r0 + size, c] = (resid[r0:r0 + size, c].astype(jnp.float32) + add).astype(jnp.bfloat16)
+            result[r0:r0 + size, c] = (resid[r0:r0 + size, c].astype(jnp.float32) + add).astype(jnp.bfloat16)
 
     barrier = pltpu.get_barrier_semaphore()
+    in_start()
     for l in range(layers):
         for k in range(3):
             if k < 2:
@@ -747,6 +789,7 @@
             for c in range(2):
                 pl.semaphore_signal(barrier, inc=1, device_id=(sp + step, 2 * x + c), device_id_type=MESH)
     pl.semaphore_wait(barrier, 2 * tp - 1 + 2 * (has_up + has_down))
+    in_copies()[0].wait()
 
     def pre_start(l):
         for k in range(2):
@@ -756,17 +799,19 @@
     when(zh_to)(lambda: zh_copy().start())
     tok_starts()
     halo_pass()
-    tok_copy(2).start()
+    when(1 - same)(lambda: tok_start(2))
     params_start()
     own_start(0, 0)
     own_start(0, 1)
     z_recv_step(0, 0, 1)
-    tok_relay()
+    when(same)(lambda: tok_start(2))
     z_recv_step(0, 1, 1)
+    tok_relay(0)
     own_start(0, 2)
     halo_pass_on()
+    tok_relay(1)
     z_recv_step(0, 0, 2)
-    tok_relay_late()
+    tok_relay(2)
     pre_start(1)
     z_recv_step(0, 1, 2)
     spread(0, 0)
@@ -775,9 +820,9 @@
     ih_copy().start()
     halo_waits()
     ih_wait()
+    params_wait()
     normalize(0, 0)
     normalize(0, 1)
-    params_wait()
     z_recv_step(0, 0, 3)
     z_recv_step(0, 1, 3)
     own_start(1, 0)
@@ -791,51 +836,60 @@
         if i == 0:
             a_step(0, 0)
             z_recv_step(0, 2, 2)
-    pre_start(2)
 
     for layer in range(last):
         after = layer + 1
+        z_recv_step(after, 0, 1)
         cv_relay(layer, 0)
+        z_recv_step(after, 1, 1)
         cv_relay(layer, 1)
         spread(layer, 2)
         z_recv_step(layer, 2, 3)
         spread(layer, 3)
-        z_recv_step(after, 0, 1)
+        if layer == 0:
+            pre_start(2)
+        z_recv_step(after, 0, 2)
         b_step(layer, 0)
         a_step(layer, 1)
-        z_recv_step(after, 1, 1)
-        for i in range(2):
-            cv_waits(layer, i)
-            activate(layer, i)
-        z_recv_step(after, 0, 2)
+        cv_waits(layer, 0)
+        activate(layer, 0)
+        z_recv_step(after, 1, 2)
+        own_start(after, 2)
+        cv_waits(layer, 1)
+        activate(layer, 1)
         r_step(layer, 0)
         a_step(layer, 2)
-        z_recv_step(after, 1, 2)
-        own_start(after, 2)
         if layer == 0:
             stream_sent()
         expand_wait(layer, 0)
         expand(layer, 0)
+        z_recv_step(after, 0, 3)
         b_step(layer, 1)
         a_step(layer, 3)
         r_step(layer, 1)
         spread(after, 0)
-        z_recv_step(after, 0, 3)
+        z_recv_step(after, 1, 3)
+        z_recv_step(after, 2, 1)
+        if after < last:
+            own_start(after + 1, 0)
+            own_start(after + 1, 1)
         expand_wait(layer, 1)
         expand(layer, 1)
         b_step(layer, 2)
-        z_recv_step(after, 1, 3)
-        if after < last:
-            own_start(after + 1, 0)
-            own_start(after + 1, 1)
+        if after == last:
+            spread(last, 1)
+            o_relay(0)
         r_step(layer, 2)
         expand_wait(layer, 2)
         expand(layer, 2)
         b_step(layer, 3)
         need_v(after)
         r_step(layer, 3)
-        z_recv_step(after, 2, 1)
-        spread(after, 1)
+        if after < last:
+            spread(after, 1)
+            z_recv_step(after, 2, 2)
+        else:
+            o_relay(1)
         expand_wait(layer, 3)
         for i in range(2):
             expand(layer, 3, (i,))
@@ -848,26 +902,32 @@
                     a_step(after, 0)
             else:
                 last_start(i)
-        z_recv_step(after, 2, 2)
+                if i == 0:
+                    z_recv_step(last, 2, 2)
+                    spread(last, 2)
     res_start()
     last_relay(0)
+    z_recv_step(last, 2, 3)
     last_relay(1)
-    spread(last, 2)
-    z_recv_step(last, 2, 3)
     spread(last, 3)
+    o_relay(2)
     res_wait()
     last_waits(0)
     activate(last, 0)
     last_waits(1)
+    o_relay(3)
     activate(last, 1)
     need_last()
-    finish(0)
-    finish(1)
+    for i in range(2):
+        finish(i)
+        out_copy(i).start()
     weights_sent()
     plane_sent()
     small_sent()
     conv_sent()
     when(same)(lambda: res_copy().wait_send())
+    for i in range(2):
+        out_copy(i).wait()
 
 
 def fused_call(mesh, *args):
@@ -882,7 +942,6 @@
     window = rows + 2 * halo
     most = window - 32
     dims = (n, tp, layers, ntaps, rows, width, chans)
-    vmem = pl.BlockSpec(memory_space=pltpu.VMEM)
     anys = pl.BlockSpec(memory_space=pl.ANY)
     bf, f32 = jnp.bfloat16, jnp.float32
     dma = lambda k: pltpu.SemaphoreType.DMA((k,))
@@ -891,9 +950,12 @@
     return pl.pallas_call(
         functools.partial(fused, dims),
         out_shape=jax.ShapeDtypeStruct((rows, feats), bf),
-        in_specs=[vmem, vmem, anys, anys, anys, vmem, vmem, vmem, vmem],
-        out_specs=vmem,
+        in_specs=[anys] * 9,
+        out_specs=anys,
         scratch_shapes=[
+            pltpu.VMEM((rows, feats), bf),
+            pltpu.VMEM(norm_gain.shape, f32),
+            pltpu.VMEM((rows, feats), bf),
             pltpu.VMEM((layers, 2, width, lch), bf),
             pltpu.VMEM((layers, n, chans, width // n), bf),
             pltpu.VMEM(conv_taps.shape, f32),
@@ -909,13 +971,13 @@
             pltpu.VMEM((rows, feats), bf),
             pltpu.VMEM((window, 128), f32),
             pltpu.VMEM((window, 128), f32),
-            dma(3 * layers),
+            dma(3 * layers), dma(6), dma(2),
             *pairs(2 * layers),
             *pairs(2 * layers * 3 * (planes - 1)),
             dma(layers * 3 * slots * 2), dma(layers * (1 + slots)),
             *pairs(wide), *pairs(wide), *pairs(wide),
-            *pairs(2 * slots),
-            *pairs(tp + 1), *pairs(tp), *pairs(3), *pairs(1),
+            *pairs(2 * slots), dma(2),
+            dma(10), dma(2 * tp), *pairs(tp), *pairs(3), *pairs(1),
             *pairs(2), dma(6), dma(2 * tp),
             *pairs(2 * layers), *pairs(2 * layers), *pairs(2 * layers),
             *pairs(6), *pairs(2 * tp), *pairs(1),

time: 117 us -> 113 us (0.966)
  the two profiles are of different devices: /device:TPU:0 before, /device:TPU:7 now
where the time goes in v3:
time: 113 us; the launch traced here: 112 us
  Pallas kernels  111 us (98%)
  local copies, waits for them, and re-layouts  1.77 us (2%)
    pallas_call x1, Pallas kernels, fused_call(): pl.pallas_call(functools.partial(fused, dims), out_shape=jax.ShapeDtypeSt...  111 us

profile of v3, /device:TPU:7, one launch (start us, length us, event | category | flops | bytes accessed | tf_op | source)
XLA Modules:
  0.0 112.4 jit_solution(17319811737573864849)
XLA Ops:
  0.0 110.6 %shard_map.91 = bf16[384,512]{1,0:T(8,128)(2,1)} custom-call(bf16[384,512]{1,0:T(8,128)(2,1)} %tok_in.1, f32[3,2048]{1,0:T(4,128)} %gain_hbm.1, bf16[3,256,256]{2,1,0:T(8,128)(2,1)} %wv_in.1, bf16[3,256,256]{2,1,0:T(8,128)(2,1)} %wg_in.1, bf16[3,256,256]{2,1,0:T(8,128)(2,1)} %wo_in.1, f32[3,31,256]{2,1,0:T(8,128)} %taps_in.1, f32[3,256]{1,0:T(4,128)} %bias_in.1, ...), custom_call_target="tpu_custom_call" | custom-call | tf_op jit(solution)/shard_map/pallas_call | solution.py:950
  110.6 1.8 %copy.11 = bf16[384,512]{1,0:T(8,128)(2,1)} copy(bf16[384,512]{1,0:T(8,128)(2,1)} %shard_map.91) | data formatting | bytes 786432

commit v4 on v3

--- a/solution.py
+++ b/solution.py
@@ -102,7 +102,7 @@
     lanes = 128
     per_side = lch // lanes
     per_out = feats // ocols
-    swapped = 1
+    swapped = 0
 
     sp = lax.axis_index("sp")
     t = lax.axis_index("tp")
@@ -123,9 +123,7 @@
 
     def route(l, slot):
         if (slot + 1) // 2 < swapped:
-            if l == 0:
-                return (x, yn), ydev, (xn, y), xdev
-            return (xn, y), xdev, (x, yn), ydev
+            return (x, yn), ydev, (xn, y), xdev
         return (ax, ay), adev, (bx, by), bdev
 
     def rcopy(src, dst, ssem, rsem, dev):
@@ -215,7 +213,8 @@
                     b_copy(l, slot, zs).start()
                 else:
                     when(differs(zs, t))(lambda: o_copy(slot, 0, zs).start())
-                    when(1 - differs(zs // 2, x))(lambda: o_copy(slot, 1, zs).start())
+                    far = 1 if s == planes - 1 else 1 - differs(zs // 2, x)
+                    when(far)(lambda: o_copy(slot, 1, zs).start())
             guarded(flag, go)
 
     def o_pass(c):
@@ -229,7 +228,8 @@
             for c in range(2):
                 owner = 2 * xn + c
                 arrived(oblock(last, t, y, owner), o_send.at[0], o_recv.at[2 * owner])
-                o_pass(c).start()
+                if s < planes - 1:
+                    o_pass(c).start()
 
     def spread_sent(l, k, slot, zs):
         if k < 2:
@@ -240,7 +240,8 @@
             d_copy(l, k, 0, slot, item(l, k, zs)).wait_send()
         else:
             when(differs(zs, t))(lambda: o_copy(slot, 0, zs).wait_send())
-            when(1 - differs(zs // 2, x))(lambda: o_copy(slot, 1, zs).wait_send())
+            far = 1 if slot > slots - 3 else 1 - differs(zs // 2, x)
+            when(far)(lambda: o_copy(slot, 1, zs).wait_send())
 
     def own_start(l, k):
         if k < 2:
@@ -320,8 +321,8 @@
             other = lax.rem(t + j, tp)
             arrived(oblock(last, t, yn, other), o_send.at[0], o_recv.at[2 * other + 1])
 
-    def weights_sent():
-        for l in range(layers):
+    def weights_sent(some):
+        for l in some:
             for k in range(3):
                 if k < 2:
                     when(1 - same)(lambda l=l, k=k: pre_copy(l, k).wait_send())
@@ -333,9 +334,13 @@
                     for flag, slot, zs in groups(s):
                         guarded(flag, lambda l=l, k=k, slot=slot, zs=zs: spread_sent(l, k, slot, zs))
 
+    def passes_sent():
+        @when(differs(jnp.abs(z - t), planes - 1))
+        def _():
+            for c in range(2):
+                o_pass(c).wait_send()
+
     def plane_sent():
-        for c in range(2):
-            o_pass(c).wait_send()
         for l in range(last):
             for s in range(planes):
                 for flag, slot, zs in groups(s):
@@ -624,6 +629,9 @@
             for l in range(last):
                 for j in range(3):
                     cv_copy(l, i, j).wait_send()
+
+    def last_sent():
+        for i in range(2):
             when(1 - same)(lambda i=i: l_copy(i, 0).wait_send())
 
             @when(same)
@@ -803,11 +811,12 @@
     params_start()
     own_start(0, 0)
     own_start(0, 1)
+    when(same)(lambda: own_start(0, 2))
     z_recv_step(0, 0, 1)
     when(same)(lambda: tok_start(2))
     z_recv_step(0, 1, 1)
     tok_relay(0)
-    own_start(0, 2)
+    when(1 - same)(lambda: own_start(0, 2))
     halo_pass_on()
     tok_relay(1)
     z_recv_step(0, 0, 2)
@@ -837,8 +846,22 @@
             a_step(0, 0)
             z_recv_step(0, 2, 2)
 
-    for layer in range(last):
+    def layer_end(layer):
         after = layer + 1
+        expand_wait(layer, 3)
+        for i in range(2):
+            expand(layer, 3, (i,))
+            normalize(after, i)
+            project(after, i)
+            convolve(after, i)
+            if after < last:
+                cv_start(after, i)
+            else:
+                last_start(i)
+
+    for layer in range(last - 1):
+        after = layer + 1
+        beyond = layer + 2
         z_recv_step(after, 0, 1)
         cv_relay(layer, 0)
         z_recv_step(after, 1, 1)
@@ -866,52 +889,80 @@
         z_recv_step(after, 0, 3)
         b_step(layer, 1)
         a_step(layer, 3)
+        z_recv_step(after, 1, 3)
         r_step(layer, 1)
         spread(after, 0)
-        z_recv_step(after, 1, 3)
         z_recv_step(after, 2, 1)
-        if after < last:
-            own_start(after + 1, 0)
-            own_start(after + 1, 1)
+        own_start(beyond, 2)
+        own_start(beyond, 0)
+        own_start(beyond, 1)
         expand_wait(layer, 1)
         expand(layer, 1)
         b_step(layer, 2)
-        if after == last:
-            spread(last, 1)
-            o_relay(0)
         r_step(layer, 2)
         expand_wait(layer, 2)
         expand(layer, 2)
         b_step(layer, 3)
         need_v(after)
         r_step(layer, 3)
-        if after < last:
-            spread(after, 1)
-            z_recv_step(after, 2, 2)
-        else:
-            o_relay(1)
-        expand_wait(layer, 3)
-        for i in range(2):
-            expand(layer, 3, (i,))
-            normalize(after, i)
-            project(after, i)
-            convolve(after, i)
-            if after < last:
-                cv_start(after, i)
-                if i == 0:
-                    a_step(after, 0)
-            else:
-                last_start(i)
-                if i == 0:
-                    z_recv_step(last, 2, 2)
-                    spread(last, 2)
+        spread(after, 1)
+        z_recv_step(after, 2, 2)
+        layer_end(layer)
+        a_step(after, 0)
+
+    layer = last - 1
+    z_recv_step(layer, 2, 3)
+    z_recv_step(last, 2, 1)
+    cv_relay(layer, 0)
+    z_recv_step(last, 0, 1)
+    cv_relay(layer, 1)
+    spread(layer, 2)
+    spread(layer, 3)
+    z_recv_step(last, 2, 2)
+    b_step(layer, 0)
+    a_step(layer, 1)
+    z_recv_step(last, 1, 1)
+    cv_waits(layer, 0)
+    activate(layer, 0)
+    z_recv_step(last, 0, 2)
+    cv_waits(layer, 1)
+    activate(layer, 1)
+    r_step(layer, 0)
+    a_step(layer, 2)
+    z_recv_step(last, 2, 3)
+    expand_wait(layer, 0)
+    expand(layer, 0)
+    z_recv_step(last, 1, 2)
+    b_step(layer, 1)
+    a_step(layer, 3)
+    r_step(layer, 1)
+    spread(last, 0)
+    spread(last, 1)
+    z_recv_step(last, 0, 3)
+    expand_wait(layer, 1)
+    expand(layer, 1)
+    spread(last, 2)
+    spread(last, 3)
+    b_step(layer, 2)
+    r_step(layer, 2)
+    z_recv_step(last, 1, 3)
+    o_relay(0)
+    expand_wait(layer, 2)
+    expand(layer, 2)
+    b_step(layer, 3)
+    need_v(last)
+    o_relay(1)
+    r_step(layer, 3)
+    layer_end(layer)
     res_start()
+    o_relay(2)
     last_relay(0)
-    z_recv_step(last, 2, 3)
     last_relay(1)
-    spread(last, 3)
-    o_relay(2)
     res_wait()
+    weights_sent(range(last))
+    plane_sent()
+    small_sent()
+    conv_sent()
     last_waits(0)
     activate(last, 0)
     last_waits(1)
@@ -921,10 +972,9 @@
     for i in range(2):
         finish(i)
         out_copy(i).start()
-    weights_sent()
-    plane_sent()
-    small_sent()
-    conv_sent()
+    weights_sent([last])
+    passes_sent()
+    last_sent()
     when(same)(lambda: res_copy().wait_send())
     for i in range(2):
         out_copy(i).wait()

time: 113 us -> 109 us (0.965)
  the two profiles are of different devices: /device:TPU:7 before, /device:TPU:0 now
where the time goes in v4:
time: 109 us; the launch traced here: 108 us
  Pallas kernels  106 us (97%)
  local copies, waits for them, and re-layouts  1.77 us (2%)
    pallas_call x1, Pallas kernels, fused_call(): pl.pallas_call(functools.partial(fused, dims), out_shape=jax.ShapeDtypeSt...  106 us

profile of v4, /device:TPU:0, one launch (start us, length us, event | category | flops | bytes accessed | tf_op | source)
XLA Modules:
  0.0 107.6 jit_solution(17956059465259664773)
XLA Ops:
  0.0 105.8 %shard_map.91 = bf16[384,512]{1,0:T(8,128)(2,1)} custom-call(bf16[384,512]{1,0:T(8,128)(2,1)} %tok_in.1, f32[3,2048]{1,0:T(4,128)} %gain_hbm.1, bf16[3,256,256]{2,1,0:T(8,128)(2,1)} %wv_in.1, bf16[3,256,256]{2,1,0:T(8,128)(2,1)} %wg_in.1, bf16[3,256,256]{2,1,0:T(8,128)(2,1)} %wo_in.1, f32[3,31,256]{2,1,0:T(8,128)} %taps_in.1, f32[3,256]{1,0:T(4,128)} %bias_in.1, ...), custom_call_target="tpu_custom_call" | custom-call | tf_op jit(solution)/shard_map/pallas_call | solution.py:1000
  105.8 1.8 %copy.11 = bf16[384,512]{1,0:T(8,128)(2,1)} copy(bf16[384,512]{1,0:T(8,128)(2,1)} %shard_map.91) | data formatting | bytes 786432

commit v5 on v4

--- a/solution.py
+++ b/solution.py
@@ -81,10 +81,10 @@
     out,
     tok, gain_in, result, wvg, wo, taps, bias, lng, lns, stream, normed, gated, cv, cv2, act, resid, rowa, rowb,
     loc_sem, in_sem, out_sem, pre_send, pre_recv, z_send, z_recv, d_send, d_recv,
-    a_send, a_recv, b_send, b_recv, r_send, r_recv, o_send, o_recv, op_send,
+    a_send, a_recv, b_send, b_recv, r_send, r_recv, o_send, o_recv,
     tok_send, tok_recv, zh_send, zh_recv, hp_send, hp_recv, ih_send, ih_recv,
     par_send, par_recv, ln_send, ln_recv,
-    ca_send, ca_recv, cb_send, cb_recv, cr_send, cr_recv,
+    cv_send, ca_recv, cb_recv, cr_recv,
     l_send, l_recv, p_send, p_recv, res_send, res_recv,
 ):
     n, tp, layers, ntaps, rows, width, chans = dims
@@ -97,12 +97,10 @@
     grain = 16
     halo = grain * layers
     window = rows + 2 * halo
-    slots = 2 * planes - 1
     last = layers - 1
     lanes = 128
     per_side = lch // lanes
     per_out = feats // ocols
-    swapped = 0
 
     sp = lax.axis_index("sp")
     t = lax.axis_index("tp")
@@ -121,11 +119,6 @@
     adev = (2 * z + ay, 2 * ax + h)
     bdev = (2 * z + by, 2 * bx + h)
 
-    def route(l, slot):
-        if (slot + 1) // 2 < swapped:
-            return (x, yn), ydev, (xn, y), xdev
-        return (ax, ay), adev, (bx, by), bdev
-
     def rcopy(src, dst, ssem, rsem, dev):
         return pltpu.make_async_remote_copy(
             src_ref=src, dst_ref=dst, send_sem=ssem, recv_sem=rsem,
@@ -134,6 +127,9 @@
     def arrived(ref, ssem, rsem):
         rcopy(ref, ref, ssem, rsem, partner).wait_recv()
 
+    def sent(ref, ssem):
+        rcopy(ref, ref, ssem, ssem, partner).wait_send()
+
     def when(flag):
         return pl.when(flag == 1)
 
@@ -155,72 +151,70 @@
     def pre_copy(l, k):
         src = (wv_in, wg_in)[k].at[l]
         i = 2 * l + k
-        return rcopy(src, vblock(l, k, z, y), pre_send.at[i], pre_recv.at[i], (spn, 2 * x + hn))
+        return rcopy(src, vblock(l, k, z, y), pre_send.at[0], pre_recv.at[i], (spn, 2 * x + hn))
+
+    def z_parts(l, k, d, s):
+        zs = z - s if d == 0 else z + s
+        return item(l, k, zs), z_recv.at[(l * 3 + k) * (planes - 1) + zs - d]
 
     def z_copy(l, k, d, s):
-        zs = z - s if d == 0 else z + s
-        ref = item(l, k, zs)
-        i = ((d * layers + l) * 3 + k) * (planes - 1) + s
-        return rcopy(ref, ref, z_send.at[i], z_recv.at[i], (sp + (2 if d == 0 else -2), t))
+        ref, rsem = z_parts(l, k, d, s)
+        return rcopy(ref, ref, z_send.at[d * (planes - 1) + s], rsem, (sp + (2 if d == 0 else -2), t))
 
     def z_wait(l, k, d, s):
-        zs = z - s if d == 0 else z + s
-        i = ((d * layers + l) * 3 + k) * (planes - 1) + s - 1
-        arrived(item(l, k, zs), z_send.at[i], z_recv.at[i])
-
-    def d_copy(l, k, src_kind, slot, ref):
-        i = ((l * 3 + k) * slots + slot) if src_kind == 0 else (
-            layers * 3 * slots + ((l * 3) + src_kind - 1) * slots + slot)
-        return rcopy(ref, ref, d_send.at[i], d_recv.at[l if k < 2 else layers + l * slots + slot], partner)
-
-    def a_copy(l, slot, zs):
-        ref, i = oblock(l, zs, y, t), l * slots + slot
-        return rcopy(ref, ref, a_send.at[i], a_recv.at[i], route(l, slot)[1])
-
-    def b_copy(l, slot, zs):
-        ref, i = oblock(l, zs, y, t), l * slots + slot
-        return rcopy(ref, ref, b_send.at[i], b_recv.at[i], route(l, slot)[3])
-
-    def from_a(l, slot, zs):
-        px, py = route(l, slot)[0]
-        return oblock(l, zs, py, 2 * px + h)
-
-    def from_b(l, slot, zs):
-        px, py = route(l, slot)[2]
-        return oblock(l, zs, py, 2 * px + h)
-
-    def r_copy(l, slot, zs):
-        ref, i = from_a(l, slot, zs), l * slots + slot
-        return rcopy(ref, ref, r_send.at[i], r_recv.at[i], route(l, slot)[3])
-
-    def o_copy(slot, rel, zs):
-        ref, i = oblock(last, zs, y, t), 2 * slot + rel
-        return rcopy(ref, ref, o_send.at[i], o_recv.at[2 * t + rel],
+        ref, rsem = z_parts(l, k, d, s)
+        arrived(ref, z_send.at[0], rsem)
+
+    def d_copy(l, k, zs, ref):
+        i, j = (l, l) if k < 2 else (layers + l, layers + l * planes + zs)
+        return rcopy(ref, ref, d_send.at[i], d_recv.at[j], partner)
+
+    def a_copy(l, zs):
+        ref = oblock(l, zs, y, t)
+        return rcopy(ref, ref, a_send.at[l], a_recv.at[l * planes + zs], adev)
+
+    def b_copy(l, zs):
+        ref = oblock(l, zs, y, t)
+        return rcopy(ref, ref, b_send.at[l], b_recv.at[l * planes + zs], bdev)
+
+    def from_a(l, zs):
+        return oblock(l, zs, ay, 2 * ax + h)
+
+    def from_b(l, zs):
+        return oblock(l, zs, by, 2 * bx + h)
+
+    def r_copy(l, zs):
+        ref = from_a(l, zs)
+        return rcopy(ref, ref, r_send.at[l], r_recv.at[l * planes + zs], bdev)
+
+    def o_copy(rel, zs):
+        ref = oblock(last, zs, y, t)
+        return rcopy(ref, ref, o_send.at[rel], o_recv.at[2 * t + rel],
                      (sp if rel == 0 else spn, zs))
 
     def differs(a, b):
         return jnp.minimum(jnp.abs(a - b), 1)
 
-    def to_partner(l, k, slot, zs):
+    def to_partner(l, k, zs):
         if k < 2 or l < last:
-            d_copy(l, k, 0, slot, item(l, k, zs)).start()
+            d_copy(l, k, zs, item(l, k, zs)).start()
 
     def spread(l, s):
-        for flag, slot, zs in groups(s):
-            def go(slot=slot, zs=zs):
+        for flag, zs in groups(s):
+            def go(zs=zs):
                 if l < last:
-                    a_copy(l, slot, zs).start()
-                    b_copy(l, slot, zs).start()
+                    a_copy(l, zs).start()
+                    b_copy(l, zs).start()
                 else:
-                    when(differs(zs, t))(lambda: o_copy(slot, 0, zs).start())
+                    when(differs(zs, t))(lambda: o_copy(0, zs).start())
                     far = 1 if s == planes - 1 else 1 - differs(zs // 2, x)
-                    when(far)(lambda: o_copy(slot, 1, zs).start())
+                    when(far)(lambda: o_copy(1, zs).start())
             guarded(flag, go)
 
     def o_pass(c):
         owner = 2 * xn + c
         ref = oblock(last, t, y, owner)
-        return rcopy(ref, ref, op_send.at[c], o_recv.at[2 * owner + 1], ydev)
+        return rcopy(ref, ref, o_send.at[2], o_recv.at[2 * owner + 1], ydev)
 
     def o_relay(s):
         @when(1 - differs(jnp.abs(z - t), s))
@@ -231,18 +225,6 @@
                 if s < planes - 1:
                     o_pass(c).start()
 
-    def spread_sent(l, k, slot, zs):
-        if k < 2:
-            d_copy(l, k, 0, slot, item(l, k, zs)).wait_send()
-        elif l < last:
-            a_copy(l, slot, zs).wait_send()
-            b_copy(l, slot, zs).wait_send()
-            d_copy(l, k, 0, slot, item(l, k, zs)).wait_send()
-        else:
-            when(differs(zs, t))(lambda: o_copy(slot, 0, zs).wait_send())
-            far = 1 if slot > slots - 3 else 1 - differs(zs // 2, x)
-            when(far)(lambda: o_copy(slot, 1, zs).wait_send())
-
     def own_start(l, k):
         if k < 2:
             when(same)(lambda: local_copy(l, k).wait())
@@ -250,12 +232,12 @@
             @when(1 - same)
             def _():
                 i = 2 * l + k
-                arrived(item(l, k, z), pre_send.at[i], pre_recv.at[i])
+                arrived(item(l, k, z), pre_send.at[0], pre_recv.at[i])
         else:
             local_copy(l, k).wait()
         when(has_up)(lambda: z_copy(l, k, 0, 0).start())
         when(has_down)(lambda: z_copy(l, k, 1, 0).start())
-        to_partner(l, k, 0, z)
+        to_partner(l, k, z)
 
     def below(s):
         return jnp.minimum(z // s, 1)
@@ -265,8 +247,8 @@
 
     def groups(s):
         if s == 0:
-            return [(None, 0, z)]
-        return [(below(s), 2 * s - 1, z - s), (above(s), 2 * s, z + s)]
+            return [(None, z)]
+        return [(below(s), z - s), (above(s), z + s)]
 
     def guarded(flag, f):
         if flag is None:
@@ -275,44 +257,44 @@
             when(flag)(f)
 
     def z_recv_step(l, k, s):
-        for d, (flag, slot, zs) in enumerate(groups(s)):
-            def go(d=d, slot=slot, zs=zs):
+        for d, (flag, zs) in enumerate(groups(s)):
+            def go(d=d, zs=zs):
                 z_wait(l, k, d, s)
                 if s < planes - 1:
                     when((has_up, has_down)[d])(lambda: z_copy(l, k, d, s).start())
-                to_partner(l, k, slot, zs)
+                to_partner(l, k, zs)
             guarded(flag, go)
 
     def a_step(l, s):
-        for flag, slot, zs in groups(s):
-            def go(slot=slot, zs=zs):
-                i = l * slots + slot
-                ref = from_a(l, slot, zs)
-                arrived(ref, a_send.at[i], a_recv.at[i])
-                r_copy(l, slot, zs).start()
-                d_copy(l, 2, 1, slot, ref).start()
+        for flag, zs in groups(s):
+            def go(zs=zs):
+                ref = from_a(l, zs)
+                arrived(ref, a_send.at[0], a_recv.at[l * planes + zs])
+                r_copy(l, zs).start()
+                d_copy(l, 2, zs, ref).start()
             guarded(flag, go)
 
     def b_step(l, s):
-        for flag, slot, zs in groups(s):
-            def go(slot=slot, zs=zs):
-                i = l * slots + slot
-                ref = from_b(l, slot, zs)
-                arrived(ref, b_send.at[i], b_recv.at[i])
-                d_copy(l, 2, 2, slot, ref).start()
+        for flag, zs in groups(s):
+            def go(zs=zs):
+                ref = from_b(l, zs)
+                arrived(ref, b_send.at[0], b_recv.at[l * planes + zs])
+                d_copy(l, 2, zs, ref).start()
             guarded(flag, go)
 
     def r_step(l, s):
-        for flag, slot, zs in groups(s):
-            def go(slot=slot, zs=zs):
-                i = l * slots + slot
+        for flag, zs in groups(s):
+            def go(zs=zs):
                 ref = oblock(l, zs, yn, 2 * xn + h)
-                arrived(ref, r_send.at[i], r_recv.at[i])
-                d_copy(l, 2, 3, slot, ref).start()
+                arrived(ref, r_send.at[0], r_recv.at[l * planes + zs])
+                d_copy(l, 2, zs, ref).start()
             guarded(flag, go)
 
+    def v_half(l):
+        return wvg.at[l, :, pl.ds(0, width // 2), :]
+
     def need_v(l):
-        arrived(wvg.at[l, :, pl.ds(0, width // 2), :], d_send.at[0], d_recv.at[l])
+        arrived(v_half(l), d_send.at[0], d_recv.at[l])
 
     def need_last():
         mate = 2 * x + hn
@@ -321,35 +303,32 @@
             other = lax.rem(t + j, tp)
             arrived(oblock(last, t, yn, other), o_send.at[0], o_recv.at[2 * other + 1])
 
-    def weights_sent(some):
-        for l in some:
-            for k in range(3):
-                if k < 2:
-                    when(1 - same)(lambda l=l, k=k: pre_copy(l, k).wait_send())
-                for s in range(planes - 1):
-                    for d, flag in enumerate((has_up, has_down)):
-                        ok = flag if s == 0 else flag * (below(s), above(s))[d]
-                        when(ok)(lambda l=l, k=k, d=d, s=s: z_copy(l, k, d, s).wait_send())
-                for s in range(planes):
-                    for flag, slot, zs in groups(s):
-                        guarded(flag, lambda l=l, k=k, slot=slot, zs=zs: spread_sent(l, k, slot, zs))
-
-    def passes_sent():
-        @when(differs(jnp.abs(z - t), planes - 1))
-        def _():
-            for c in range(2):
-                o_pass(c).wait_send()
-
-    def plane_sent():
+    def v_sent():
+        when(1 - same)(lambda: sent(wvg.at[:, :, pl.ds(0, krows), :], pre_send.at[0]))
+        for l in range(layers):
+            sent(v_half(l), d_send.at[l])
+        for s in range(planes - 1):
+            for d, flag in enumerate((has_up, has_down)):
+                ok = flag if s == 0 else flag * (below(s), above(s))[d]
+                ref = wvg.at[:, :, pl.ds(0, 3 * krows // 2), :]
+                when(ok)(lambda d=d, s=s, ref=ref: sent(ref, z_send.at[d * (planes - 1) + s]))
+
+    def o_sent():
         for l in range(last):
-            for s in range(planes):
-                for flag, slot, zs in groups(s):
-                    def go(l=l, slot=slot, zs=zs):
-                        r_copy(l, slot, zs).wait_send()
-                        d_copy(l, 2, 1, slot, from_a(l, slot, zs)).wait_send()
-                        d_copy(l, 2, 2, slot, from_b(l, slot, zs)).wait_send()
-                        d_copy(l, 2, 3, slot, oblock(l, zs, yn, 2 * xn + h)).wait_send()
-                    guarded(flag, go)
+            sent(wo.at[l, pl.ds(0, planes)], d_send.at[layers + l])
+            for sem in (a_send, b_send, r_send):
+                sent(wo.at[l, 0], sem.at[l])
+
+    def o_last_sent():
+        def some(i, count):
+            sent(wo.at[last, 0, pl.ds(0, count * lch), :], o_send.at[i])
+
+        at_end = 1 - differs(jnp.abs(planes - 1 - 2 * z), planes - 1)
+        extra = at_end * differs((planes - 1 - z) // 2, x)
+        some(0, tp - 1)
+        when(extra)(lambda: some(1, 3))
+        when(1 - extra)(lambda: some(1, 2))
+        when(differs(jnp.abs(z - t), planes - 1))(lambda: some(2, 2))
 
     def cols(owner):
         return pl.ds(pl.multiple_of(owner * feats, feats), feats)
@@ -364,7 +343,7 @@
     def tok_copy(j, p):
         dev = ((sp, 2 * x + y), (sp, 2 * xn + y), (spn, 2 * x + y))[j]
         return rcopy(tok.at[pl.ds(p * half_rows, half_rows), :], hcols(t, p),
-                     tok_send.at[2 * j + p], tok_recv.at[2 * t + p], dev)
+                     tok_send.at[min(j, 1)], tok_recv.at[2 * t + p], dev)
 
     def tok_start(j):
         tok_copy(j, 0).start()
@@ -375,7 +354,7 @@
             (2 * xn + yn, 0, ydev), (2 * x + yn, 0, xdev),
             (2 * x + yn, 1, xdev), (2 * x + y, 1, xdev))[j]
         ref = hcols(owner, p)
-        return rcopy(ref, ref, tok_send.at[6 + j], tok_recv.at[2 * owner + p], dev)
+        return rcopy(ref, ref, tok_send.at[2], tok_recv.at[2 * owner + p], dev)
 
     def tok_starts():
         when(1 - same)(lambda: tok_start(0))
@@ -431,7 +410,7 @@
 
     def zh_copy():
         src = tok.at[pl.ds(pl.multiple_of(y * (rows - halo), grain), halo), :]
-        return rcopy(src, edge(tcols, yn), zh_send.at[0], zh_recv.at[t],
+        return rcopy(src, edge(tcols, yn), zh_send.at[0], zh_recv.at[0],
                      (sp + 4 * y - 2, 2 * x + yn))
 
     def half_cols(xx):
@@ -439,13 +418,12 @@
 
     def hp_copy(j):
         ref = edge(half_cols(xn if j == 2 else x), h)
-        return rcopy(ref, ref, hp_send.at[j], hp_recv.at[j], xdev if j == 0 else ydev)
+        return rcopy(ref, ref, hp_send.at[0], hp_recv.at[j], xdev if j == 0 else ydev)
 
     def halo_pass():
         @when(zh_from * (1 - same))
         def _():
-            for c in range(2):
-                arrived(edge(cols(2 * x + c), h), zh_send.at[0], zh_recv.at[2 * x + c])
+            arrived(edge(half_cols(x), h), zh_send.at[0], zh_recv.at[0])
             hp_copy(0).start()
             hp_copy(1).start()
 
@@ -480,7 +458,7 @@
 
     def ln_copy(i, j):
         a, b = ((lng_in, lng), (lns_in, lns))[i]
-        return rcopy(a, b.at[t], ln_send.at[3 * i + j - 1], ln_recv.at[tp * i + t],
+        return rcopy(a, b.at[t], ln_send.at[i], ln_recv.at[i],
                      (sp, lax.rem(t + j, tp)))
 
     def params_start():
@@ -519,33 +497,22 @@
         for i, ref in enumerate((taps, bias)):
             when(1 - same)(lambda i=i, ref=ref: arrived(ref, par_send.at[i], par_recv.at[i]))
         for i, ref in enumerate((lng, lns)):
-            for j in range(1, tp):
-                other = lax.rem(t + j, tp)
-                arrived(ref.at[other], ln_send.at[0], ln_recv.at[tp * i + other])
+            arrived(ref.at[pl.ds(0, tp - 1)], ln_send.at[0], ln_recv.at[i])
 
     def small_sent():
-        for p in range(2):
-            when(1 - same)(lambda p=p: tok_copy(0, p).wait_send())
-            tok_copy(1, p).wait_send()
-            tok_copy(2, p).wait_send()
+        when(1 - same)(lambda: sent(tok, tok_send.at[0]))
+        sent(stream.at[pl.ds(0, rows), pl.ds(0, 2 * feats)], tok_send.at[1])
         when(zh_to)(lambda: zh_copy().wait_send())
-        for i in range(2):
+        for i, ref in enumerate((lng, lns)):
             when(same)(lambda i=i: par_copy(i).wait_send())
-            for j in range(1, tp):
-                ln_copy(i, j).wait_send()
+            sent(ref.at[pl.ds(0, tp - 1)], ln_send.at[i])
 
     def stream_sent():
-        when(same)(lambda: tok_pass(0).wait_send())
-
-        @when(1 - same)
-        def _():
-            for j in range(1, 4):
-                tok_pass(j).wait_send()
-
-        @when(zh_from * (1 - same))
-        def _():
-            for j in range(3):
-                hp_copy(j).wait_send()
+        for flag, count in ((same, 1), (1 - same, 3)):
+            ref = stream.at[pl.ds(0, half_rows), pl.ds(0, count * feats)]
+            when(flag)(lambda ref=ref: sent(ref, tok_send.at[2]))
+        ref = stream.at[pl.ds(0, 3 * halo), pl.ds(0, 2 * feats)]
+        when(zh_from * (1 - same))(lambda: sent(ref, hp_send.at[0]))
         ih_copy().wait_send()
 
     cb_own = 2 * x + y
@@ -562,20 +529,20 @@
 
     def cv_copy(l, i, j):
         ref = cblock(l, i, cb_a if j == 2 else cb_own)
-        s, r = ((ca_send, ca_recv), (cb_send, cb_recv), (cr_send, cr_recv))[j]
-        return rcopy(ref, ref, s.at[2 * l + i], r.at[2 * l + i], adev if j == 0 else bdev)
+        r = (ca_recv, cb_recv, cr_recv)[j]
+        return rcopy(ref, ref, cv_send.at[l], r.at[2 * l + i], adev if j == 0 else bdev)
 
     def cv_start(l, i):
         cv_copy(l, i, 0).start()
         cv_copy(l, i, 1).start()
 
     def cv_relay(l, i):
-        arrived(cblock(l, i, cb_a), ca_send.at[2 * l + i], ca_recv.at[2 * l + i])
+        arrived(cblock(l, i, cb_a), cv_send.at[0], ca_recv.at[2 * l + i])
         cv_copy(l, i, 2).start()
 
     def cv_waits(l, i):
-        arrived(cblock(l, i, cb_b), cb_send.at[2 * l + i], cb_recv.at[2 * l + i])
-        arrived(cblock(l, i, cb_d), cr_send.at[2 * l + i], cr_recv.at[2 * l + i])
+        arrived(cblock(l, i, cb_b), cv_send.at[0], cb_recv.at[2 * l + i])
+        arrived(cblock(l, i, cb_d), cv_send.at[0], cr_recv.at[2 * l + i])
 
     def lblock(i, cb):
         r0, size = piece(last, i)
@@ -587,12 +554,12 @@
             (cblock(last, i, cb_own), cb_own, xdev),
             (lblock(i, 2 * x + yn), 2 * x + yn, xdev),
         )[j]
-        return rcopy(src, lblock(i, cb), l_send.at[3 * i + j], l_recv.at[3 * i + j], dev)
+        return rcopy(src, lblock(i, cb), l_send.at[0], l_recv.at[3 * i + j], dev)
 
     def p_copy(i, j):
         cb = (cb_own, 2 * x + yn, 2 * xn + y, 2 * xn + yn)[j]
         src = cblock(last, i, cb) if j == 0 else lblock(i, cb)
-        return rcopy(src, lblock(i, cb), p_send.at[tp * i + j], p_recv.at[tp * i + j], partner)
+        return rcopy(src, lblock(i, cb), p_send.at[0], p_recv.at[i], partner)
 
     def last_start(i):
         r0, size = piece(last, i)
@@ -619,27 +586,21 @@
                 arrived(lblock(i, cb), l_send.at[0], l_recv.at[3 * i + j])
                 p_copy(i, j + 1).start()
 
-        @when(1 - same)
-        def _():
-            for j, cb in enumerate((2 * x + yn, 2 * x + y, 2 * xn + yn, 2 * xn + y)):
-                arrived(lblock(i, cb), p_send.at[0], p_recv.at[tp * i + j])
+        r0, size = piece(last, i)
+        when(1 - same)(lambda: arrived(cv2.at[:, pl.ds(r0, size), :], p_send.at[0], p_recv.at[i]))
 
     def conv_sent():
-        for i in range(2):
-            for l in range(last):
-                for j in range(3):
-                    cv_copy(l, i, j).wait_send()
+        for l in range(last):
+            total = window - 2 * grain * (l + 1)
+            sent(cv.at[l, pl.ds(0, 3), pl.ds(0, total), :], cv_send.at[l])
 
     def last_sent():
-        for i in range(2):
-            when(1 - same)(lambda i=i: l_copy(i, 0).wait_send())
-
-            @when(same)
-            def _(i=i):
-                l_copy(i, 1).wait_send()
-                l_copy(i, 2).wait_send()
-                for j in range(tp):
-                    p_copy(i, j).wait_send()
+        when(1 - same)(lambda: sent(cv2.at[0], l_send.at[0]))
+
+        @when(same)
+        def _():
+            sent(cv2.at[pl.ds(0, 2)], l_send.at[0])
+            sent(cv2, p_send.at[0])
 
     def res_copy():
         src = stream.at[pl.ds(halo, rows), cols(2 * x + hn)]
@@ -753,13 +714,13 @@
         over_rows(r0, size, block, apply)
 
     def expand_wait(layer, s):
-        for flag, slot, zs in groups(s):
-            sem = d_recv.at[layers + layer * slots + slot]
+        for flag, zs in groups(s):
+            sem = d_recv.at[layers + layer * planes + zs]
             guarded(flag, lambda sem=sem: arrived(wo.at[layer, 0], d_send.at[0], sem))
 
     def expand(layer, s, pieces=(0, 1)):
-        for flag, slot, zs in groups(s):
-            def go(slot=slot, zs=zs):
+        for flag, zs in groups(s):
+            def go(zs=zs):
                 def step(j, carry):
                     c = pl.ds(pl.multiple_of((2 * zs + j) * ocols, ocols), ocols)
                     for i in pieces:
@@ -846,7 +807,7 @@
             a_step(0, 0)
             z_recv_step(0, 2, 2)
 
-    def layer_end(layer):
+    def layer_end(layer, between):
         after = layer + 1
         expand_wait(layer, 3)
         for i in range(2):
@@ -858,6 +819,8 @@
                 cv_start(after, i)
             else:
                 last_start(i)
+            if i == 0:
+                between()
 
     for layer in range(last - 1):
         after = layer + 1
@@ -906,8 +869,7 @@
         need_v(after)
         r_step(layer, 3)
         spread(after, 1)
-        z_recv_step(after, 2, 2)
-        layer_end(layer)
+        layer_end(layer, lambda: z_recv_step(after, 2, 2))
         a_step(after, 0)
 
     layer = last - 1
@@ -953,14 +915,13 @@
     need_v(last)
     o_relay(1)
     r_step(layer, 3)
-    layer_end(layer)
+    layer_end(layer, lambda: None)
     res_start()
     o_relay(2)
     last_relay(0)
     last_relay(1)
     res_wait()
-    weights_sent(range(last))
-    plane_sent()
+    o_sent()
     small_sent()
     conv_sent()
     last_waits(0)
@@ -972,8 +933,8 @@
     for i in range(2):
         finish(i)
         out_copy(i).start()
-    weights_sent([last])
-    passes_sent()
+    v_sent()
+    o_last_sent()
     last_sent()
     when(same)(lambda: res_copy().wait_send())
     for i in range(2):
@@ -987,7 +948,7 @@
     rows, feats = tokens.shape
     width, chans = feats * tp, lch * tp
     planes = n // 2
-    slots = 2 * planes - 1
+    last = layers - 1
     halo = 16 * layers
     window = rows + 2 * halo
     most = window - 32
@@ -995,8 +956,6 @@
     anys = pl.BlockSpec(memory_space=pl.ANY)
     bf, f32 = jnp.bfloat16, jnp.float32
     dma = lambda k: pltpu.SemaphoreType.DMA((k,))
-    pairs = lambda k: [dma(k), dma(k)]
-    wide = (layers - 1) * slots
     return pl.pallas_call(
         functools.partial(fused, dims),
         out_shape=jax.ShapeDtypeStruct((rows, feats), bf),
@@ -1022,15 +981,15 @@
             pltpu.VMEM((window, 128), f32),
             pltpu.VMEM((window, 128), f32),
             dma(3 * layers), dma(6), dma(2),
-            *pairs(2 * layers),
-            *pairs(2 * layers * 3 * (planes - 1)),
-            dma(layers * 3 * slots * 2), dma(layers * (1 + slots)),
-            *pairs(wide), *pairs(wide), *pairs(wide),
-            *pairs(2 * slots), dma(2),
-            dma(10), dma(2 * tp), *pairs(tp), *pairs(3), *pairs(1),
-            *pairs(2), dma(6), dma(2 * tp),
-            *pairs(2 * layers), *pairs(2 * layers), *pairs(2 * layers),
-            *pairs(6), *pairs(2 * tp), *pairs(1),
+            dma(1), dma(2 * layers),
+            dma(2 * (planes - 1)), dma(3 * layers * (planes - 1)),
+            dma(layers + last), dma(layers + last * planes),
+            *[dma(k) for _ in range(3) for k in (last, last * planes)],
+            dma(3), dma(2 * tp),
+            dma(3), dma(2 * tp), dma(1), dma(1), dma(1), dma(3), dma(1), dma(1),
+            dma(2), dma(2), dma(2), dma(2),
+            dma(last), dma(2 * last), dma(2 * last), dma(2 * last),
+            dma(1), dma(6), dma(1), dma(2), dma(1), dma(1),
         ],
         compiler_params=pltpu.CompilerParams(
             collective_id=0, has_side_effects=True, vmem_limit_bytes=60 * 1024 * 1024),

time: 109 us -> 105 us (0.963)
  Pallas kernels: 106 us -> 103 us
    pallas_call x1, Pallas kernels: 106 us -> 103 us  [fused_call(): pl.pallas_call(functools.partial(fused, dims), out_shape=jax.ShapeDtypeSt...]
where the time goes in v5:
time: 105 us; the launch traced here: 104 us
  Pallas kernels  103 us (98%)
  local copies, waits for them, and re-layouts  1.77 us (2%)
    pallas_call x1, Pallas kernels, fused_call(): pl.pallas_call(functools.partial(fused, dims), out_shape=jax.ShapeDtypeSt...  103 us

profile of v5, /device:TPU:0, one launch (start us, length us, event | category | flops | bytes accessed | tf_op | source)
XLA Modules:
  0.0 104.4 jit_solution(8868108182547357354)
XLA Ops:
  0.0 102.7 %shard_map.91 = bf16[384,512]{1,0:T(8,128)(2,1)} custom-call(bf16[384,512]{1,0:T(8,128)(2,1)} %tok_in.1, f32[3,2048]{1,0:T(4,128)} %gain_hbm.1, bf16[3,256,256]{2,1,0:T(8,128)(2,1)} %wv_in.1, bf16[3,256,256]{2,1,0:T(8,128)(2,1)} %wg_in.1, bf16[3,256,256]{2,1,0:T(8,128)(2,1)} %wo_in.1, f32[3,31,256]{2,1,0:T(8,128)} %taps_in.1, f32[3,256]{1,0:T(4,128)} %bias_in.1, ...), custom_call_target="tpu_custom_call" | custom-call | tf_op jit(solution)/shard_map/pallas_call | solution.py:959
  102.7 1.8 %copy.11 = bf16[384,512]{1,0:T(8,128)(2,1)} copy(bf16[384,512]{1,0:T(8,128)(2,1)} %shard_map.91) | data formatting | bytes 786432

commit v6 on v5

--- a/solution.py
+++ b/solution.py
@@ -788,13 +788,18 @@
     z_recv_step(0, 2, 1)
     tok_waits()
     ih_copy().start()
+
+    def first_weights_in():
+        z_recv_step(0, 0, 3)
+        z_recv_step(0, 1, 3)
+
+    when(same)(first_weights_in)
     halo_waits()
     ih_wait()
     params_wait()
     normalize(0, 0)
     normalize(0, 1)
-    z_recv_step(0, 0, 3)
-    z_recv_step(0, 1, 3)
+    when(1 - same)(first_weights_in)
     own_start(1, 0)
     own_start(1, 1)
     spread(0, 1)
@@ -900,11 +905,11 @@
     r_step(layer, 1)
     spread(last, 0)
     spread(last, 1)
+    spread(last, 2)
+    spread(last, 3)
     z_recv_step(last, 0, 3)
     expand_wait(layer, 1)
     expand(layer, 1)
-    spread(last, 2)
-    spread(last, 3)
     b_step(layer, 2)
     r_step(layer, 2)
     z_recv_step(last, 1, 3)
@@ -928,11 +933,12 @@
     activate(last, 0)
     last_waits(1)
     o_relay(3)
+    need_last()
+    finish(0)
+    out_copy(0).start()
     activate(last, 1)
-    need_last()
-    for i in range(2):
-        finish(i)
-        out_copy(i).start()
+    finish(1)
+    out_copy(1).start()
     v_sent()
     o_last_sent()
     last_sent()

time: 105 us -> 105 us (level)
  no operation moved by 1% of the time
where the time goes in v6:
time: 105 us; the launch traced here: 104 us
  Pallas kernels  102 us (97%)
  local copies, waits for them, and re-layouts  1.77 us (2%)
    pallas_call x1, Pallas kernels, fused_call(): pl.pallas_call(functools.partial(fused, dims), out_shape=jax.ShapeDtypeSt...  102 us

profile of v6, /device:TPU:0, one launch (start us, length us, event | category | flops | bytes accessed | tf_op | source)
XLA Modules:
  0.0 103.7 jit_solution(6802793532623796858)
XLA Ops:
  0.0 102.0 %shard_map.91 = bf16[384,512]{1,0:T(8,128)(2,1)} custom-call(bf16[384,512]{1,0:T(8,128)(2,1)} %tok_in.1, f32[3,2048]{1,0:T(4,128)} %gain_hbm.1, bf16[3,256,256]{2,1,0:T(8,128)(2,1)} %wv_in.1, bf16[3,256,256]{2,1,0:T(8,128)(2,1)} %wg_in.1, bf16[3,256,256]{2,1,0:T(8,128)(2,1)} %wo_in.1, f32[3,31,256]{2,1,0:T(8,128)} %taps_in.1, f32[3,256]{1,0:T(4,128)} %bias_in.1, ...), custom_call_target="tpu_custom_call" | custom-call | tf_op jit(solution)/shard_map/pallas_call | solution.py:965
  102.0 1.8 %copy.11 = bf16[384,512]{1,0:T(8,128)(2,1)} copy(bf16[384,512]{1,0:T(8,128)(2,1)} %shard_map.91) | data formatting | bytes 786432

commit v7 on v6

--- a/solution.py
+++ b/solution.py
@@ -80,7 +80,7 @@
     tok_in, gain_hbm, wv_in, wg_in, wo_in, taps_in, bias_in, lng_in, lns_in,
     out,
     tok, gain_in, result, wvg, wo, taps, bias, lng, lns, stream, normed, gated, cv, cv2, act, resid, rowa, rowb,
-    loc_sem, in_sem, out_sem, pre_send, pre_recv, z_send, z_recv, d_send, d_recv,
+    loc_sem, in_sem, out_sem, pre_send, z_send, z_recv, d_send, d_recv,
     a_send, a_recv, b_send, b_recv, r_send, r_recv, o_send, o_recv,
     tok_send, tok_recv, zh_send, zh_recv, hp_send, hp_recv, ih_send, ih_recv,
     par_send, par_recv, ln_send, ln_recv,
@@ -150,8 +150,7 @@
 
     def pre_copy(l, k):
         src = (wv_in, wg_in)[k].at[l]
-        i = 2 * l + k
-        return rcopy(src, vblock(l, k, z, y), pre_send.at[0], pre_recv.at[i], (spn, 2 * x + hn))
+        return rcopy(src, vblock(l, k, z, y), pre_send.at[0], loc_sem.at[3 * l + k], (spn, 2 * x + hn))
 
     def z_parts(l, k, d, s):
         zs = z - s if d == 0 else z + s
@@ -231,8 +230,7 @@
 
             @when(1 - same)
             def _():
-                i = 2 * l + k
-                arrived(item(l, k, z), pre_send.at[0], pre_recv.at[i])
+                arrived(item(l, k, z), pre_send.at[0], loc_sem.at[3 * l + k])
         else:
             local_copy(l, k).wait()
         when(has_up)(lambda: z_copy(l, k, 0, 0).start())
@@ -837,8 +835,6 @@
         spread(layer, 2)
         z_recv_step(layer, 2, 3)
         spread(layer, 3)
-        if layer == 0:
-            pre_start(2)
         z_recv_step(after, 0, 2)
         b_step(layer, 0)
         a_step(layer, 1)
@@ -846,6 +842,8 @@
         activate(layer, 0)
         z_recv_step(after, 1, 2)
         own_start(after, 2)
+        if layer == 0:
+            pre_start(2)
         cv_waits(layer, 1)
         activate(layer, 1)
         r_step(layer, 0)
@@ -987,7 +985,7 @@
             pltpu.VMEM((window, 128), f32),
             pltpu.VMEM((window, 128), f32),
             dma(3 * layers), dma(6), dma(2),
-            dma(1), dma(2 * layers),
+            dma(1),
             dma(2 * (planes - 1)), dma(3 * layers * (planes - 1)),
             dma(layers + last), dma(layers + last * planes),
             *[dma(k) for _ in range(3) for k in (last, last * planes)],

time: 105 us -> 105 us (level)
  no operation moved by 1% of the time
where the time goes in v7:
time: 105 us; the launch traced here: 104 us
  Pallas kernels  102 us (97%)
  local copies, waits for them, and re-layouts  1.77 us (2%)
    pallas_call x1, Pallas kernels, fused_call(): pl.pallas_call(functools.partial(fused, dims), out_shape=jax.ShapeDtypeSt...  102 us

profile of v7, /device:TPU:0, one launch (start us, length us, event | category | flops | bytes accessed | tf_op | source)
XLA Modules:
  0.0 103.9 jit_solution(701527445561746677)
XLA Ops:
  0.0 102.1 %shard_map.91 = bf16[384,512]{1,0:T(8,128)(2,1)} custom-call(bf16[384,512]{1,0:T(8,128)(2,1)} %tok_in.1, f32[3,2048]{1,0:T(4,128)} %gain_hbm.1, bf16[3,256,256]{2,1,0:T(8,128)(2,1)} %wv_in.1, bf16[3,256,256]{2,1,0:T(8,128)(2,1)} %wg_in.1, bf16[3,256,256]{2,1,0:T(8,128)(2,1)} %wo_in.1, f32[3,31,256]{2,1,0:T(8,128)} %taps_in.1, f32[3,256]{1,0:T(4,128)} %bias_in.1, ...), custom_call_target="tpu_custom_call" | custom-call | tf_op jit(solution)/shard_map/pallas_call | solution.py:963
  102.1 1.8 %copy.11 = bf16[384,512]{1,0:T(8,128)(2,1)} copy(bf16[384,512]{1,0:T(8,128)(2,1)} %shard_map.91) | data formatting | bytes 786432
